TPU v7x, 32 devices: a whole 2x2x4 slice. The times are simulated.
32 devices in a mesh: sp: 8 (over z, core), tp: 4 (over y, x).
Axes of the slice: x: 2, y: 2, z: 4, core: 2. Of those that a mesh axis runs over, the one named last changes fastest.
Arguments:
- resid: bfloat16 [2048, 2048], P('sp'), may hold values from -18 to 18
- narrow_head_input: bfloat16 [2048, 1024], P('sp', 'tp'), may hold values from -6 to 6
- wide_head_input: bfloat16 [2048, 2048], P('sp', 'tp'), may hold values from -6 to 6
- key_group_input: bfloat16 [2048, 512], P('sp'), may hold values from -6 to 6
- query_group_input: bfloat16 [2048, 512], P('sp'), may hold values from -6 to 6
- narrow_output_gate: bfloat16 [2048, 1024], P('sp', 'tp'), may hold values from -6 to 6
- wide_output_gate: bfloat16 [2048, 2048], P('sp', 'tp'), may hold values from -6 to 6
- step_input_rows: bfloat16 [2048, 2, 16], P('sp', None, 'tp'), may hold values from -4 to 4
- head_decay_logarithm: float32 [2, 16], P(None, 'tp'), may hold values from -14 to -2
- position_log_decay: float32 [2048, 2, 16], P('sp', None, 'tp'), may hold values from -1.4 to 0
- direct_input_weight: float32 [2, 16], P(None, 'tp'), may hold values from 0.5 to 2
- narrow_conv_taps: float32 [4, 1024], P(None, 'tp'), may hold values from -3 to 3
- wide_conv_taps: float32 [4, 2048], P(None, 'tp'), may hold values from -3 to 3
- key_conv_taps: float32 [4, 512], replicated, may hold values from -3 to 3
- query_conv_taps: float32 [4, 512], replicated, may hold values from -3 to 3
- narrow_norm_gain: float32 [1024], P('tp'), may hold values from 0.1 to 1.9
- wide_norm_gain: float32 [2048], P('tp'), may hold values from 0.1 to 1.9
- narrow_output_rows: bfloat16 [1024, 2048], P('tp'), may hold values from -0.109375 to 0.109375
- wide_output_rows: bfloat16 [2048, 2048], P('tp'), may hold values from -0.109375 to 0.109375
- feedforward_norm_gain: float32 [2048], replicated, may hold values from 0.1 to 1.9
- routes: int32 [2048, 3], P('sp'), may hold values from 0 to 7, all different within a row; in each aligned block of 256 rows (0 to 255, 256 to 511, ...) at most 128 rows name the same one
- routing_weight_values: float32 [2048, 3], P('sp'), may hold values from 0.1 to 1
- expert_gate_matrix: bfloat16 [8, 2048, 2048], P('sp', None, 'tp'), may hold values from -1 to 1
- expert_up_matrix: bfloat16 [8, 2048, 2048], P('sp', None, 'tp'), may hold values from -1 to 1
- expert_down_matrix: bfloat16 [8, 2048, 2048], P('sp', 'tp'), may hold values from -0.015625 to 0.015625
Outputs:
- layer_out: bfloat16 [2048, 2048], P('sp', 'tp')
Inputs may be any that keep to these rules, and one draw needn't show every extreme that they name: `routes`: each token names 3 different experts. Among the tokens of one index of sp (aligned blocks of 256 rows) no expert is named by more than 128 of them, and in some blocks one is named by exactly 128.
All inputs are finite; a program needn't handle non-finite values.
Results may differ from a plain program's by a relative error of at most 0.015.
Values may be sent and summed in bfloat16 or wider, within the bound.
A program may use at most 64 MiB of HBM per device.

v0:
```python
import functools

import jax
import jax.numpy as jnp
from jax import lax
from jax.sharding import PartitionSpec as P

HEADS = 16
NARROW_HEAD_DIM = 64
WIDE_HEAD_DIM = 128
GROUPS = 4
BLOCK = 128


NORM_EPS = 1e-06
CLAMP_LIMIT = 7.0
SIGMOID_SCALE = 1.702
FULL_PRECISION = lax.Precision.HIGHEST


def passed_along(block, axis, distance):
    devices = range(lax.axis_size(axis))
    route = [(i - distance, i) for i in devices if i - distance in devices]
    return lax.ppermute(block, axis, route)


def entering_2(x, axis, join, neutral):
    place = lax.axis_index(axis)
    gathered = jax.tree.map(
        lambda a, kind: lax.all_gather(a.astype(kind), axis),
        x,
        jax.tree.map(lambda a: jnp.bfloat16 if a.dtype == jnp.float32 else a.dtype, x),
    )
    state = jax.tree.map(lambda a, e: jnp.zeros_like(a) + jnp.asarray(e, a.dtype), x, neutral)

    def one(lap, state):
        return join(
            state,
            jax.tree.map(
                lambda a, own: lax.dynamic_index_in_dim(a, lap, 0, False).astype(own.dtype),
                gathered,
                x,
            ),
        )

    return lax.fori_loop(0, place, one, state)


def conv_with_rim(values, rim_rows, weight):
    length = values.shape[0]
    padded = jnp.concatenate([rim_rows, values], axis=0).astype(jnp.float32)
    accumulated = jnp.zeros((length, values.shape[1]), jnp.float32)
    for tap_index in range(weight.shape[0]):
        accumulated = accumulated + weight[tap_index] * padded[tap_index : tap_index + length]
    return jax.nn.silu(accumulated)


def pick_groups(channel_table, first_head, head_count):
    length = channel_table.shape[0]
    grouped = channel_table.reshape(length, GROUPS, -1)
    owners = (first_head + jnp.arange(head_count, dtype=jnp.int32)) // (HEADS // GROUPS)
    chooser = (owners[:, None] == jnp.arange(GROUPS, dtype=jnp.int32)[None, :]).astype(jnp.float32)
    return jnp.einsum("sgn,hg->shn", grouped, chooser, precision=FULL_PRECISION)


def local_head(values, step_logarithm, key_head_rows, query_head_rows, block_len):
    block_count = values.shape[0] // block_len
    values = values.reshape(block_count, block_len, -1)
    step_logarithm = step_logarithm.reshape(block_count, block_len)
    key_head_rows = key_head_rows.reshape(block_count, block_len, -1)
    query_head_rows = query_head_rows.reshape(block_count, block_len, -1)
    cum_decay = jnp.cumsum(step_logarithm, axis=1)
    causal_mask = jnp.arange(block_len)[:, None] >= jnp.arange(block_len)[None, :]
    decay_gaps = jnp.where(causal_mask[None], cum_decay[:, :, None] - cum_decay[:, None, :], -1e30)
    scores = jnp.einsum(
        "bln,bsn->bls", query_head_rows, key_head_rows, precision=FULL_PRECISION
    ) * jnp.exp(decay_gaps)
    inside = jnp.einsum("bls,bsp->blp", scores, values, precision=FULL_PRECISION)
    tail_decay = jnp.exp(cum_decay[:, -1:] - cum_decay)
    states = jnp.einsum(
        "bln,blp->bnp", key_head_rows * tail_decay[..., None], values, precision=FULL_PRECISION
    )
    totals = cum_decay[:, -1]

    def walk(running, member):
        return (jnp.exp(member[1]) * running + member[0], running)

    closing, entering = lax.scan(walk, jnp.zeros(states.shape[1:], jnp.float32), (states, totals))
    before = jnp.cumsum(totals) - totals
    return (inside, entering, closing, jnp.sum(totals), before, cum_decay, query_head_rows)


def finish_head(inside, entering, before, cum_decay, query_blocks, carried):
    starting = entering + jnp.exp(before)[:, None, None] * carried[None]
    readout = jnp.einsum(
        "bln,bnp->blp",
        query_blocks * jnp.exp(cum_decay)[..., None],
        starting,
        precision=FULL_PRECISION,
    )
    return (inside + readout).reshape(-1, inside.shape[-1])


def group_out(scanned, mixed_input_rows, direct_input_term, gate_input_rows, norm_gain_vector):
    length, head_count, head_dimension = mixed_input_rows.shape
    gated = jax.nn.silu(gate_input_rows.astype(jnp.float32)).reshape(
        length, head_count, head_dimension
    )
    result = (scanned + direct_input_term[None, :, None] * mixed_input_rows) * gated
    result = result * lax.rsqrt(jnp.mean(result * result, axis=-1, keepdims=True) + NORM_EPS)
    return (result.reshape(length, head_count * head_dimension) * norm_gain_vector).astype(
        jnp.bfloat16
    )


def head_pieces_list(
    mixed_input_rows,
    step_length_values,
    decay_vector,
    position_decay_rows,
    key_head_rows,
    query_head_rows,
):
    step_logarithm = -jnp.exp(decay_vector)[None, :] * step_length_values + position_decay_rows
    values = mixed_input_rows * step_length_values[..., None]
    walker = functools.partial(local_head, block_len=BLOCK)
    return jax.vmap(walker, in_axes=(1, 1, 1, 1))(
        values, step_logarithm, key_head_rows, query_head_rows
    )


def finish_group(parts, carried_states):
    return jax.vmap(finish_head, in_axes=(0, 0, 0, 0, 0, 0), out_axes=1)(
        parts[0], parts[1], parts[4], parts[5], parts[6], carried_states
    )


def chain_combine(earlier, later):
    return (
        earlier[0] + later[0],
        earlier[1] + later[1],
        jnp.exp(later[0])[:, None, None] * earlier[2] + later[2],
        jnp.exp(later[1])[:, None, None] * earlier[3] + later[3],
    )


def local(
    resid,
    narrow_head_input,
    wide_head_input,
    key_group_input,
    query_group_input,
    narrow_output_gate,
    wide_output_gate,
    step_input_rows,
    head_decay_logarithm,
    position_log_decay,
    direct_input_weight,
    narrow_conv_taps,
    wide_conv_taps,
    key_conv_taps,
    query_conv_taps,
    narrow_norm_gain,
    wide_norm_gain,
    narrow_output_rows,
    wide_output_rows,
    feedforward_norm_gain,
    routes,
    routing_weight_values,
    expert_gate_matrix,
    expert_up_matrix,
    expert_down_matrix,
):
    length = resid.shape[0]
    head_count = narrow_head_input.shape[1] // NARROW_HEAD_DIM
    rim_len = narrow_conv_taps.shape[0] - 1
    rim_rows = passed_along(
        (
            narrow_head_input[length - rim_len :],
            wide_head_input[length - rim_len :],
            key_group_input[length - rim_len :],
            query_group_input[length - rim_len :],
        ),
        "sp",
        1,
    )
    narrow_head_mix = conv_with_rim(narrow_head_input, rim_rows[0], narrow_conv_taps).reshape(
        length, head_count, NARROW_HEAD_DIM
    )
    wide_head_mix = conv_with_rim(wide_head_input, rim_rows[1], wide_conv_taps).reshape(
        length, head_count, WIDE_HEAD_DIM
    )
    first_head = lax.axis_index("tp") * head_count
    key_head_rows = pick_groups(
        conv_with_rim(key_group_input, rim_rows[2], key_conv_taps), first_head, head_count
    )
    query_head_rows = pick_groups(
        conv_with_rim(query_group_input, rim_rows[3], query_conv_taps), first_head, head_count
    )
    step_length_values = jax.nn.softplus(step_input_rows.astype(jnp.float32))
    narrow_parts = head_pieces_list(
        narrow_head_mix,
        step_length_values[:, 0],
        head_decay_logarithm[0],
        position_log_decay[:, 0],
        key_head_rows,
        query_head_rows,
    )
    wide_parts = head_pieces_list(
        wide_head_mix,
        step_length_values[:, 1],
        head_decay_logarithm[1],
        position_log_decay[:, 1],
        key_head_rows,
        query_head_rows,
    )
    summary = (narrow_parts[3], wide_parts[3], narrow_parts[2], wide_parts[2])
    carried = entering_2(
        summary,
        "sp",
        chain_combine,
        (
            jnp.zeros_like(summary[0]),
            jnp.zeros_like(summary[1]),
            jnp.zeros_like(summary[2]),
            jnp.zeros_like(summary[3]),
        ),
    )
    narrow_carry, wide_carry = (carried[2], carried[3])
    narrow_head_output = group_out(
        finish_group(narrow_parts, narrow_carry),
        narrow_head_mix,
        direct_input_weight[0],
        narrow_output_gate,
        narrow_norm_gain,
    )
    wide_head_output = group_out(
        finish_group(wide_parts, wide_carry),
        wide_head_mix,
        direct_input_weight[1],
        wide_output_gate,
        wide_norm_gain,
    )
    partial_mix = jnp.dot(
        narrow_head_output, narrow_output_rows, preferred_element_type=jnp.float32
    )
    partial_mix = partial_mix + jnp.dot(
        wide_head_output, wide_output_rows, preferred_element_type=jnp.float32
    )
    mixed = lax.psum(partial_mix.astype(jnp.bfloat16), "tp").astype(jnp.float32)
    hidden_state = resid.astype(jnp.float32) + mixed
    normed = (
        hidden_state
        * lax.rsqrt(jnp.mean(hidden_state * hidden_state, axis=-1, keepdims=True) + NORM_EPS)
        * feedforward_norm_gain
    ).astype(jnp.bfloat16)
    experts = lax.axis_size("sp")
    picks = routes.shape[1]
    capacity = 4 * length * picks // (3 * experts)
    column_width = normed.shape[1] // lax.axis_size("tp")
    tp_index = lax.axis_index("tp")
    flat_routes = routes.reshape(-1)
    member_hits = (flat_routes[:, None] == jnp.arange(experts, dtype=jnp.int32)[None, :]).astype(
        jnp.int32
    )
    ranks = jnp.sum((jnp.cumsum(member_hits, axis=0) - member_hits) * member_hits, axis=1)
    slot_ids = flat_routes * capacity + ranks
    source_rows = (
        jnp.zeros((experts * capacity,), jnp.int32)
        .at[slot_ids]
        .set(jnp.arange(length * picks, dtype=jnp.int32) // picks)
    )
    occupied = jnp.zeros((experts * capacity,), jnp.int32).at[slot_ids].set(1)
    gate_weight = expert_gate_matrix[0]
    up_weight = expert_up_matrix[0]
    down_weight = expert_down_matrix[0]
    own_columns = lax.dynamic_slice_in_dim(normed, tp_index * column_width, column_width, 1)
    outgoing = jnp.where(
        occupied[:, None] > 0, own_columns[source_rows], jnp.zeros((), jnp.bfloat16)
    )
    arrived = lax.all_to_all(
        outgoing.reshape(experts, capacity, column_width),
        "sp",
        split_axis=0,
        concat_axis=0,
        tiled=True,
    )
    slot_parts = arrived.reshape(experts * capacity, column_width)
    piece = lax.all_gather(slot_parts, "tp", axis=1, tiled=True)
    gate_pre = jnp.dot(piece, gate_weight, preferred_element_type=jnp.float32)
    up_pre = jnp.dot(piece, up_weight, preferred_element_type=jnp.float32)
    clamped = jnp.minimum(gate_pre, CLAMP_LIMIT)
    act = (
        (jnp.clip(up_pre, -CLAMP_LIMIT, CLAMP_LIMIT) + 1.0)
        * clamped
        * jax.nn.sigmoid(SIGMOID_SCALE * clamped)
    ).astype(jnp.bfloat16)
    partial_out = jnp.dot(act, down_weight, preferred_element_type=jnp.float32)
    summed = lax.psum_scatter(
        partial_out.reshape(experts, capacity, -1).astype(jnp.bfloat16),
        "tp",
        scatter_dimension=2,
        tiled=True,
    )
    returned = lax.all_to_all(summed, "sp", split_axis=0, concat_axis=0, tiled=True)
    token_rows = returned.reshape(experts * capacity, -1)[slot_ids].reshape(length, picks, -1)
    combined = jnp.sum(token_rows.astype(jnp.float32) * routing_weight_values[..., None], axis=1)
    own_state = lax.dynamic_slice_in_dim(hidden_state, tp_index * column_width, column_width, 1)
    return (own_state + combined).astype(jnp.bfloat16)


def solution(mesh):
    return jax.shard_map(
        local,
        mesh=mesh,
        in_specs=(
            P("sp", None),
            P("sp", "tp"),
            P("sp", "tp"),
            P("sp", None),
            P("sp", None),
            P("sp", "tp"),
            P("sp", "tp"),
            P("sp", None, "tp"),
            P(None, "tp"),
            P("sp", None, "tp"),
            P(None, "tp"),
            P(None, "tp"),
            P(None, "tp"),
            P(),
            P(),
            P("tp"),
            P("tp"),
            P("tp", None),
            P("tp", None),
            P(),
            P("sp", None),
            P("sp", None),
            P("sp", None, "tp"),
            P("sp", None, "tp"),
            P("sp", "tp", None),
        ),
        out_specs=P("sp", "tp"),
        check_vma=False,
    )
```

profile of v0, /device:TPU:0, one launch (start us, length us, event | category | flops | bytes accessed | tf_op | source)
XLA Modules:
  0.0 406.6 jit_solution(8500874269213244223)
XLA Ops:
  6.5 1.4 slice.156
  8.0 3.0 collective-permute-start.1
  11.8 4.6 %collective-permute-start.2 = (bf16[3,256]{0,1:T(8,128)(2,1)S(1)}, bf16[3,256]{0,1:T(8,128)(2,1)}, u32[]{:S(2)}, u32[]{:S(2)}) collective-permute-start(bf16[3,256]{0,1:T(8,128)(2,1)S(1)} %copy.90), channel_id=1, source_target_pairs={{0,4},{4,8},{8,12},{12,16},{16,20},{20,24},{24,28},{1,5},{5,9},{9,... | collective-permute-start | bytes 4616 | tf_op jit(solution)/shard_map/ppermute | solution.py:24
  16.4 1.3 slice.182
  17.7 1.9 collective-permute-start.3
  19.6 1.3 slice.147
  20.9 3.6 collective-permute-start
  24.5 1.7 copy.91
  33.9 1.5 fusion.104
  35.9 1.4 fusion.108
  37.4 1.5 fusion.103
  38.8 1.5 fusion.102
  40.9 1.3 slice_bitcast_fusion.2
  46.2 13.6 %all-reduce.2 = (bf16[32]{0:T(256)(128)(2,1)S(1)}, bf16[32]{0:T(256)(128)(2,1)S(1)}) all-reduce(bf16[32]{0:T(256)(128)(2,1)S(1)} %dynamic-update-slice, bf16[32]{0:T(256)(128)(2,1)S(1)} %dynamic-update-slice.1), channel_id=2, replica_groups=mesh['sp'=8,'tp'=4] {'sp'}, use_global_device_ids=true, to_apply=%add | all-reduce | flops 64 | bytes 256
  66.6 1.8 divide_multiply_fusion.3
  72.5 1.8 divide_multiply_fusion
  75.5 1.5 multiply_bitcast_fusion
  77.1 2.1 copy.128
  79.1 3.0 broadcast_multiply_fusion.2
  83.2 3.1 while.44
  87.0 1.7 convolution_bitcast_fusion.1
  88.7 3.4 while.43
  94.6 17.4 %all-gather.1 = bf16[32,128,64]{1,2,0:T(8,128)(2,1)} all-gather(bf16[4,128,64]{1,2,0:T(8,128)(2,1)S(1)} %copy.100), channel_id=3, replica_groups=mesh['sp'=8,'tp'=4] {'sp'}, dimensions={0}, use_global_device_ids=true | all-gather | bytes 589824 | tf_op jit(solution)/shard_map/all_gather | solution.py:30
  112.1 3.0 broadcast_multiply_fusion.1
  117.1 1.6 fusion.43
  119.0 2.9 convolution_add_fusion.1
  121.9 2.0 copy.117
  124.0 1.5 multiply_reduce_fusion.2
  130.5 1.7 fusion.10
  132.5 1.7 reduce-window.6
  135.1 3.4 scatter_custom_fusion.1
  138.5 3.4 scatter_custom_fusion
  142.7 60.3 %all-reduce.5.cloned.1.call-done = bf16[256,2048]{1,0:T(8,128)(2,1)} async-done(((bf16[256,2048]{1,0:T(8,128)(2,1)}), bf16[256,2048]{1,0:T(8,128)(2,1)}) %all-reduce.5.cloned.1.call-update) | async-done | bytes 1048592 | tf_op jit(solution)/shard_map/psum | solution.py:250
  203.0 1.6 multiply_reduce_fusion.1
  204.6 1.4 copy-done.3
  206.1 4.0 gather_fusion
  210.3 31.1 %all_to_all.10 = bf16[8,128,512]{2,1,0:T(8,128)(2,1)} all-to-all(bf16[8,128,512]{2,1,0:T(8,128)(2,1)S(1)} %broadcast_select_fusion), channel_id=1, replica_groups=mesh['sp'=8,'tp'=4] {'sp'}, dimensions={0} | all-to-all | bytes 2097152 | tf_op jit(solution)/shard_map/all_to_all | solution.py:281
  241.7 50.3 %all-gather.7.cloned.1.call-done = bf16[1024,2048]{1,0:T(8,128)(2,1)} async-done(((bf16[1024,512]{1,0:T(8,128)(2,1)}), bf16[1024,2048]{1,0:T(8,128)(2,1)}) %all-gather.7.cloned.1.call-update) | async-done | bytes 4194320 | tf_op jit(solution)/shard_map/all_gather | solution.py:289
  291.9 5.3 %fusion.14 = f32[1024,512]{1,0:T(8,128)S(1)} fusion(bf16[1024,2048]{1,0:T(8,128)(2,1)} %all-gather.7.cloned.1.call-done, bf16[1,2048,512]{2,1,0:T(8,128)(2,1)} %param.54), kind=kOutput, calls=%fused_computation.32 | convolution fusion | flops 2147483648 | bytes 8388608 | tf_op jit(solution)/shard_map/dot_general | solution.py:291
  297.3 2.8 multiply_convert_fusion
  300.2 4.3 %convolution_convert_fusion = bf16[8,128,2048]{2,1,0:T(8,128)(2,1)} fusion(bf16[8,128,512]{2,1,0:T(8,128)(2,1)S(1)} %bitcast.258, bf16[1,512,2048]{2,1,0:T(8,128)(2,1)S(1)} %copy-done), kind=kOutput, calls=%fused_computation.26 | convolution fusion | flops 2149580800 | bytes 7340032 | tf_op jit(solution)/shard_map/dot_general | solution.py:298
  304.5 52.7 %reduce-scatter.2.cloned.1.call-done = bf16[8,128,512]{2,1,0:T(8,128)(2,1)} async-done(((bf16[8,128,2048]{2,1,0:T(8,128)(2,1)}), bf16[8,128,512]{2,1,0:T(8,128)(2,1)}) %reduce-scatter.2.cloned.1.call-update) | async-done | bytes 1048592 | tf_op jit(solution)/shard_map/reduce_scatter | solution.py:299
  357.3 4.6 %all-to-all-start.1 = ((bf16[8,128,512]{2,1,0:T(8,128)(2,1)}), bf16[8,128,512]{2,1,0:T(8,128)(2,1)S(1)}, u32[]{:S(2)}, u32[]{:S(2)}) async-start(bf16[8,128,512]{2,1,0:T(8,128)(2,1)} %reduce-scatter.2.cloned.1.call-done), calls=%async_computation.2 | async-start | bytes 2097152 | tf_op jit(solution)/shard_map/all_to_all | solution.py:305
  362.0 26.4 %all-to-all-done.1 = bf16[8,128,512]{2,1,0:T(8,128)(2,1)S(1)} async-done(((bf16[8,128,512]{2,1,0:T(8,128)(2,1)}), bf16[8,128,512]{2,1,0:T(8,128)(2,1)S(1)}, u32[]{:S(2)}, u32[]{:S(2)}) %all-to-all-start.1) | async-done | bytes 1048608 | tf_op jit(solution)/shard_map/all_to_all | solution.py:305
  388.4 3.3 gather_fusion.1
  391.8 3.5 reshape.282
  395.2 2.9 multiply_reduce_fusion
  398.2 1.8 add_convert_fusion
  (212 shorter events, 45.4 us)
Async XLA Ops:
  6.5 293.6 %copy-start = (bf16[1,512,2048]{2,1,0:T(8,128)(2,1)S(1)}, bf16[1,512,2048]{2,1,0:T(8,128)(2,1)}, u32[]{:S(2)}) copy-start(bf16[1,512,2048]{2,1,0:T(8,128)(2,1)} %param.55) | copy-start | bytes 6291460
  6.5 57.3 %copy-start.18 = (bf16[256,256]{1,0:T(8,128)(2,1)S(1)}, bf16[256,256]{1,0:T(8,128)(2,1)}, u32[]{:S(2)}) copy-start(bf16[256,256]{1,0:T(8,128)(2,1)} %param.36) | copy-start | bytes 393220
  6.5 58.0 %copy-start.29 = (s32[256,3]{0,1:T(4,128)S(1)}, s32[256,3]{0,1:T(4,128)}, u32[]{:S(2)}) copy-start(s32[256,3]{0,1:T(4,128)} %param.51) | copy-start | bytes 9220
  6.5 112.2 %all-gather.9.cloned.1.call-start = ((), (), s32[]{:S(2)}) async-start(), calls=%async_computation.6 | async-start | bytes 1179648 | tf_op jit(solution)/shard_map/all_gather | solution.py:30
  8.0 60.4 %collective-permute-start.1 = (bf16[3,512]{1,0:T(4,128)(2,1)}, bf16[3,512]{1,0:T(4,128)(2,1)}, u32[]{:S(2)}, u32[]{:S(2)}) collective-permute-start(bf16[3,512]{1,0:T(4,128)(2,1)} %slice.156), channel_id=1, source_target_pairs={{0,4},{4,8},{8,12},{12,16},{16,20},{20,24},{24,28},{1,5},{5,9},{9,... | collective-permute-start | bytes 9224 | tf_op jit(solution)/shard_map/ppermute | solution.py:24
  11.8 53.7 %collective-permute-start.2 = (bf16[3,256]{0,1:T(8,128)(2,1)S(1)}, bf16[3,256]{0,1:T(8,128)(2,1)}, u32[]{:S(2)}, u32[]{:S(2)}) collective-permute-start(bf16[3,256]{0,1:T(8,128)(2,1)S(1)} %copy.90), channel_id=1, source_target_pairs={{0,4},{4,8},{8,12},{12,16},{16,20},{20,24},{24,28},{1,5},{5,9},{9,... | collective-permute-start | bytes 4616 | tf_op jit(solution)/shard_map/ppermute | solution.py:24
  17.7 53.7 %collective-permute-start.3 = (bf16[3,512]{1,0:T(4,128)(2,1)}, bf16[3,512]{1,0:T(4,128)(2,1)}, u32[]{:S(2)}, u32[]{:S(2)}) collective-permute-start(bf16[3,512]{1,0:T(4,128)(2,1)} %slice.182), channel_id=1, source_target_pairs={{0,4},{4,8},{8,12},{12,16},{16,20},{20,24},{24,28},{1,5},{5,9},{9,... | collective-permute-start | bytes 9224 | tf_op jit(solution)/shard_map/ppermute | solution.py:24
  20.9 71.3 %collective-permute-start = (bf16[3,512]{1,0:T(4,128)(2,1)}, bf16[3,512]{1,0:T(4,128)(2,1)}, u32[]{:S(2)}, u32[]{:S(2)}) collective-permute-start(bf16[3,512]{1,0:T(4,128)(2,1)} %slice.147), channel_id=1, source_target_pairs={{0,4},{4,8},{8,12},{12,16},{16,20},{20,24},{24,28},{1,5},{5,9},{9,... | collective-permute-start | bytes 9224 | tf_op jit(solution)/shard_map/ppermute | solution.py:24
  30.3 35.2 %copy-start.21 = (f32[4,2,128]{2,1,0:T(2,128)}, f32[4,2,128]{2,1,0:T(2,128)S(1)}, u32[]{:S(2)}) copy-start(f32[4,2,128]{2,1,0:T(2,128)S(1)} %reduce_window_sum.49) | copy-start | bytes 12292
  31.5 34.0 %copy-start.23 = (f32[4,2,128]{2,1,0:T(2,128)}, f32[4,2,128]{2,1,0:T(2,128)S(1)}, u32[]{:S(2)}) copy-start(f32[4,2,128]{2,1,0:T(2,128)S(1)} %reduce_window_sum.51) | copy-start | bytes 12292
  31.8 33.7 %copy-start.28 = (f32[4,2,1]{0,1,2:T(2,128)}, f32[4,2,1]{0,1,2:T(2,128)S(1)}, u32[]{:S(2)}) copy-start(f32[4,2,1]{0,1,2:T(2,128)S(1)} %copy.101) | copy-start | bytes 100
  32.0 33.5 %copy-start.27 = (f32[4,2,1]{0,1,2:T(2,128)}, f32[4,2,1]{0,1,2:T(2,128)S(1)}, u32[]{:S(2)}) copy-start(f32[4,2,1]{0,1,2:T(2,128)S(1)} %copy.94) | copy-start | bytes 100
  75.5 6.6 %copy-start.4 = (f32[256,512]{0,1:T(8,128)}, f32[256,512]{0,1:T(8,128)S(1)}, u32[]{:S(2)}) copy-start(f32[256,512]{0,1:T(8,128)S(1)} %copy.104) | copy-start | bytes 1572868
  79.1 3.0 copy-start.1
  86.9 116.0 %all-reduce.5.cloned.1.call-start = ((), (), s32[]{:S(2)}) async-start(), calls=%async_computation.3 | async-start | bytes 2097152 | tf_op jit(solution)/shard_map/psum | solution.py:250
  88.7 4.6 %copy-start.35 = (f32[1,512]{1,0:T(1,128)S(1)}, f32[1,512]{1,0:T(1,128)}, u32[]{:S(2)}) copy-start(f32[1,512]{1,0:T(1,128)} %get-tuple-element.285) | copy-start | bytes 6148
  88.7 4.6 %copy-start.36 = (f32[1,512]{1,0:T(1,128)S(1)}, f32[1,512]{1,0:T(1,128)}, u32[]{:S(2)}) copy-start(f32[1,512]{1,0:T(1,128)} %get-tuple-element.286) | copy-start | bytes 6148
  88.7 4.6 %copy-start.37 = (f32[1,512]{1,0:T(1,128)S(1)}, f32[1,512]{1,0:T(1,128)}, u32[]{:S(2)}) copy-start(f32[1,512]{1,0:T(1,128)} %get-tuple-element.287) | copy-start | bytes 6148
  88.7 4.6 %copy-start.38 = (f32[1,512]{1,0:T(1,128)S(1)}, f32[1,512]{1,0:T(1,128)}, u32[]{:S(2)}) copy-start(f32[1,512]{1,0:T(1,128)} %get-tuple-element.288) | copy-start | bytes 6148
  93.3 18.7 %copy-start.19 = (f32[4,2,128]{0,2,1:T(8,128)S(1)}, f32[4,2,128]{0,2,1:T(8,128)}, u32[]{:S(2)}) copy-start(f32[4,2,128]{0,2,1:T(8,128)} %copy.93) | copy-start | bytes 12292
  93.3 18.7 %copy-start.20 = (f32[4,2,128]{0,2,1:T(8,128)S(1)}, f32[4,2,128]{0,2,1:T(8,128)}, u32[]{:S(2)}) copy-start(f32[4,2,128]{0,2,1:T(8,128)} %copy.114) | copy-start | bytes 12292
  93.3 18.7 %copy-start.46 = (s32[4]{0:T(128)S(1)}, s32[4]{0:T(128)}, u32[]{:S(2)}) copy-start(s32[4]{0:T(128)} %and_select_fusion) | copy-start | bytes 52
  112.0 3.0 copy-start.14
  112.0 5.1 %copy-start.2 = (f32[4,256,128]{2,1,0:T(8,128)S(1)}, f32[4,256,128]{2,1,0:T(8,128)}, u32[]{:S(2)}) copy-start(f32[4,256,128]{2,1,0:T(8,128)} %copy.128) | copy-start | bytes 1572868
  112.1 5.0 %copy-start.24 = (f32[4,2,128]{2,1,0:T(2,128)S(1)}, f32[4,2,128]{2,1,0:T(2,128)}, u32[]{:S(2)}) copy-start(f32[4,2,128]{2,1,0:T(2,128)} %copy-done.23) | copy-start | bytes 12292
  119.0 5.0 %copy-start.5 = (f32[256,512]{0,1:T(8,128)S(1)}, f32[256,512]{0,1:T(8,128)}, u32[]{:S(2)}) copy-start(f32[256,512]{0,1:T(8,128)} %copy-done.4) | copy-start | bytes 1572868
  121.9 3.7 copy-start.40
  123.9 2.8 copy-start.7
  123.9 2.8 copy-start.8
  124.0 2.8 copy-start.22
  124.0 2.8 copy-start.25
  124.0 4.1 copy-start.15
  124.0 4.1 copy-start.31
  124.0 4.1 copy-start.32
  124.0 4.1 copy-start.33
  124.0 4.1 copy-start.34
  124.0 4.1 copy-start.41
  126.8 1.8 copy-start.42
  130.5 1.8 copy-start.26
  130.5 1.8 copy-start.11
  130.5 4.2 %copy-start.30 = (s32[256,3]{0,1:T(4,128)S(1)}, s32[256,3]{0,1:T(4,128)}, u32[]{:S(2)}) copy-start(s32[256,3]{0,1:T(4,128)} %param.51) | copy-start | bytes 9220
  132.2 70.8 %copy-start.13 = (bf16[256,2048]{1,0:T(8,128)(2,1)S(1)}, bf16[256,2048]{1,0:T(8,128)(2,1)}, u32[]{:S(2)}) copy-start(bf16[256,2048]{1,0:T(8,128)(2,1)} %param.31) | copy-start | bytes 3145732
  132.2 159.8 %all-gather.7.cloned.1.call-start = ((), (), s32[]{:S(2)}) async-start(), calls=%async_computation.4 | async-start | bytes 5242880 | tf_op jit(solution)/shard_map/all_gather | solution.py:289
  241.4 115.9 %reduce-scatter.2.cloned.1.call-start = ((), (), s32[]{:S(2)}) async-start(), calls=%async_computation.5 | async-start | bytes 5242880 | tf_op jit(solution)/shard_map/reduce_scatter | solution.py:299
  291.9 5.3 %copy-start.44 = (bf16[1024,2048]{1,0:T(8,128)(2,1)S(1)}, bf16[1024,2048]{1,0:T(8,128)(2,1)}, u32[]{:S(2)}) copy-start(bf16[1024,2048]{1,0:T(8,128)(2,1)} %all-gather.7.cloned.1.call-done) | copy-start | bytes 12582916
  291.9 5.4 %copy-start.45 = (bf16[1,2048,512]{2,1,0:T(8,128)(2,1)S(1)}, bf16[1,2048,512]{2,1,0:T(8,128)(2,1)}, u32[]{:S(2)}) copy-start(bf16[1,2048,512]{2,1,0:T(8,128)(2,1)} %param.53) | copy-start | bytes 6291460
  304.5 57.3 %copy-start.39 = (f32[256,3]{0,1:T(4,128)S(1)}, f32[256,3]{0,1:T(4,128)}, u32[]{:S(2)}) copy-start(f32[256,3]{0,1:T(4,128)} %param.52) | copy-start | bytes 9220
  357.3 31.2 %all-to-all-start.1 = ((bf16[8,128,512]{2,1,0:T(8,128)(2,1)}), bf16[8,128,512]{2,1,0:T(8,128)(2,1)S(1)}, u32[]{:S(2)}, u32[]{:S(2)}) async-start(bf16[8,128,512]{2,1,0:T(8,128)(2,1)} %reduce-scatter.2.cloned.1.call-done), calls=%async_computation.2 | async-start | bytes 2097152 | tf_op jit(solution)/shard_map/all_to_all | solution.py:305
  (8 other events, 9.9 us)
Sparse Core Ops, SparseCore 0:
  87.0 23.1 all-gather.8
  132.3 70.6 all-reduce.4
  241.5 50.3 all-gather.6
  304.7 52.5 reduce-scatter.1
where the time goes:
time: 409 us; the launch traced here: 407 us
  waiting for transfers between devices  190 us (46%)
  blocking collectives  62 us (15%)
  local copies, waits for them, and re-layouts  56.8 us (14%)
  other arithmetic  33.6 us (8%)
  matrix products  31.5 us (8%)
  starting transfers between devices  18 us (4%)
  between operations  14.6 us (4%)
    psum x1, waiting for transfers between devices, local(): mixed = lax.psum(partial_mix.astype(jnp.bfloat16), 'tp').astype(jnp.float32)  60.3 us
    reduce_scatter x1, waiting for transfers between devices, local(): lax.psum_scatter(partial_out.reshape(experts, capacity, -1).astype(jnp.bf...  52.7 us
    all_gather x1, waiting for transfers between devices, local(): piece = lax.all_gather(slot_parts, 'tp', axis=1, tiled=True)  50.3 us
    all_to_all x1, blocking collectives, local(): lax.all_to_all(outgoing.reshape(experts, capacity, column_width), 'sp', s...  31.1 us
    all_to_all x1, waiting for transfers between devices, local(): lax.all_to_all(summed, 'sp', split_axis=0, concat_axis=0, tiled=True)  26.4 us
    all_gather x1, blocking collectives, entering_2(): lax.all_gather(a.astype(kind), axis)  17.4 us
    unnamed x1, blocking collectives  13.6 us
    ppermute x4, starting transfers between devices, passed_along(): return lax.ppermute(block, axis, route)  13.1 us
  transfers between devices with their start and end apart: 9, of which 4 were waited for; matrix products, arithmetic and copies ran while one was open for 18% of the time, Pallas kernels for 0%

commit v1 on v0

--- a/solution.py
+++ b/solution.py
@@ -3,6 +3,8 @@
 import jax
 import jax.numpy as jnp
 from jax import lax
+from jax.experimental import pallas as pl
+from jax.experimental.pallas import tpu as pltpu
 from jax.sharding import PartitionSpec as P
 
 HEADS = 16
@@ -142,6 +144,440 @@
         jnp.exp(later[0])[:, None, None] * earlier[2] + later[2],
         jnp.exp(later[1])[:, None, None] * earlier[3] + later[3],
     )
+
+
+def ring_map(index, count):
+    side = int(round(count**0.5))
+    if side * side != count:
+        return index
+    row = index // side
+    column = index % side
+    return row * side + column + (row % 2) * (side - 1 - 2 * column)
+
+
+def tail_kernel(
+    shards,
+    experts,
+    narrow_ref,
+    wide_ref,
+    narrow_rows_ref,
+    wide_rows_ref,
+    resid_ref,
+    gain_ref,
+    rank_ref,
+    weight_ref,
+    gate_hbm,
+    up_hbm,
+    down_hbm,
+    out_ref,
+    gate_v,
+    up_v,
+    down_v,
+    share_out,
+    share_in,
+    square_out,
+    square_in,
+    hidden,
+    normed,
+    dispatch_out,
+    tokens,
+    partial,
+    sums,
+    done_out,
+    done_in,
+    load_sem,
+    share_send,
+    share_recv,
+    square_send,
+    square_recv,
+    dispatch_send,
+    dispatch_recv,
+    gather_send,
+    gather_recv,
+    sum_send,
+    sum_recv,
+    done_send,
+    done_recv,
+):
+    me_s = lax.axis_index("sp")
+    me_t = lax.axis_index("tp")
+    length, width = resid_ref.shape
+    capacity = done_in.shape[1]
+    groups = tokens.shape[1]
+    sources = experts // groups
+    half = tokens.shape[2] // 2
+    place = ring_map(me_t, shards)
+    after = ring_map((place + 1) % shards, shards)
+    before = ring_map((place + shards - 1) % shards, shards)
+
+    def remote(src, dst, send, recv, where):
+        return pltpu.make_async_remote_copy(
+            src_ref=src,
+            dst_ref=dst,
+            send_sem=send,
+            recv_sem=recv,
+            device_id=where,
+            device_id_type=pl.DeviceIdType.MESH,
+        )
+
+    loads = [
+        pltpu.make_async_copy(h, v, load_sem.at[i])
+        for i, (h, v) in enumerate(((gate_hbm, gate_v), (up_hbm, up_v), (down_hbm, down_v)))
+    ]
+    for load in loads:
+        load.start()
+
+    barrier = pltpu.get_barrier_semaphore()
+
+    def greet_tp(d, c):
+        pl.semaphore_signal(
+            barrier,
+            inc=1,
+            device_id=(me_s, (me_t + d) % shards),
+            device_id_type=pl.DeviceIdType.MESH,
+        )
+        return c
+
+    def greet_sp(d, c):
+        pl.semaphore_signal(
+            barrier,
+            inc=1,
+            device_id=((me_s + d) % experts, me_t),
+            device_id_type=pl.DeviceIdType.MESH,
+        )
+        return c
+
+    lax.fori_loop(1, shards, greet_tp, 0)
+    lax.fori_loop(1, experts, greet_sp, 0)
+    pl.semaphore_wait(barrier, shards + experts - 2)
+
+    def project(block):
+        columns = pl.ds(pl.multiple_of(block * width, 128), width)
+        return (
+            jnp.dot(
+                narrow_ref[...], narrow_rows_ref[:, columns], preferred_element_type=jnp.float32
+            )
+            + jnp.dot(wide_ref[...], wide_rows_ref[:, columns], preferred_element_type=jnp.float32)
+        ).astype(jnp.bfloat16)
+
+    def share_copy(d):
+        return remote(
+            share_out.at[d],
+            share_in.at[d],
+            share_send.at[d],
+            share_recv.at[d],
+            (me_s, (me_t + d) % shards),
+        )
+
+    def send_share(d, c):
+        share_out[d] = project((me_t + d) % shards)
+        share_copy(d).start()
+        return c
+
+    lax.fori_loop(1, shards, send_share, 0)
+    hidden[...] = resid_ref[...].astype(jnp.float32) + project(me_t).astype(jnp.float32)
+
+    def take_share(d, c):
+        share_copy(d).wait_recv()
+        hidden[...] += share_in[d].astype(jnp.float32)
+        return c
+
+    lax.fori_loop(1, shards, take_share, 0)
+    state = hidden[...]
+    own_square = jnp.sum(state * state, axis=1, keepdims=True)
+    square_rows = jnp.transpose(jnp.broadcast_to(own_square, (length, 128)))
+    square_out[...] = square_rows[:8]
+
+    def square_copy(d):
+        return remote(
+            square_out,
+            square_in.at[d],
+            square_send.at[d],
+            square_recv.at[d],
+            (me_s, (me_t + d) % shards),
+        )
+
+    def send_square(d, c):
+        square_copy(d).start()
+        return c
+
+    lax.fori_loop(1, shards, send_square, 0)
+
+    def take_square(d, total):
+        square_copy(d).wait_recv()
+        return total + square_in[d]
+
+    total = lax.fori_loop(1, shards, take_square, square_rows[:8])
+    scale_row = lax.rsqrt(total[:1] / (shards * width) + NORM_EPS)
+    scale = jnp.transpose(jnp.broadcast_to(scale_row, (128, length)))[:, :1]
+    normed[...] = (hidden[...] * scale * gain_ref[...]).astype(jnp.bfloat16)
+
+    slots = lax.broadcasted_iota(jnp.int32, (capacity, length), 0)
+
+    def pick(d):
+        chooser = jnp.where(slots == rank_ref[d], 1.0, 0.0).astype(jnp.bfloat16)
+        return jnp.dot(chooser, normed[...], preferred_element_type=jnp.float32).astype(
+            jnp.bfloat16
+        )
+
+    def dispatch_copy(d):
+        return remote(
+            dispatch_out.at[d],
+            tokens.at[me_t, d // sources, pl.ds((d % sources) * capacity, capacity)],
+            dispatch_send.at[d],
+            dispatch_recv.at[d],
+            ((me_s + d) % experts, me_t),
+        )
+
+    def send_dispatch(d, c):
+        dispatch_out[d] = pick(d)
+        dispatch_copy(d).start()
+        return c
+
+    tokens[me_t, 0, :capacity] = pick(0)
+    lax.fori_loop(1, experts, send_dispatch, 0)
+
+    def gather_copy(way, hop, d):
+        step_back = hop - 1 if way else shards - hop + 1
+        block = ring_map((place + step_back) % shards, shards)
+        part = tokens.at[block, d, pl.ds(way * half, half)]
+        return remote(
+            part,
+            part,
+            gather_send.at[way, hop, d],
+            gather_recv.at[way, hop, d],
+            (me_s, before if way else after),
+        )
+
+    def sum_block(way, hop):
+        if way:
+            return ring_map((place + hop) % shards, shards)
+        return ring_map((place + shards - hop) % shards, shards)
+
+    def sum_copy(way, hop, d):
+        source = sums.at[way, hop - 1, d]
+        return remote(
+            source,
+            sums.at[way, hop, d],
+            sum_send.at[way, hop, d],
+            sum_recv.at[way, hop, d],
+            (me_s, before if way else after),
+        )
+
+    def done_copy(d):
+        return remote(
+            done_out.at[d // sources, pl.ds((d % sources) * capacity, capacity)],
+            done_in.at[d],
+            done_send.at[d],
+            done_recv.at[d],
+            ((me_s + experts - d) % experts, me_t),
+        )
+
+    def expert(d):
+        gate = jnp.zeros((2 * half, gate_v.shape[1]), jnp.float32)
+        up = jnp.zeros((2 * half, gate_v.shape[1]), jnp.float32)
+        for j in range(shards):
+            rows = pl.ds(j * width, width)
+            piece = tokens[j, d]
+            gate += jnp.dot(piece, gate_v[rows, :], preferred_element_type=jnp.float32)
+            up += jnp.dot(piece, up_v[rows, :], preferred_element_type=jnp.float32)
+        clamped = jnp.minimum(gate, CLAMP_LIMIT)
+        act = (
+            (jnp.clip(up, -CLAMP_LIMIT, CLAMP_LIMIT) + 1.0)
+            * clamped
+            * jax.nn.sigmoid(SIGMOID_SCALE * clamped)
+        ).astype(jnp.bfloat16)
+        for j in range(shards):
+            partial[j, d] = jnp.dot(
+                act, down_v[:, j * width : (j + 1) * width], preferred_element_type=jnp.float32
+            ).astype(jnp.bfloat16)
+
+    last = shards - 1
+
+    def step(i, c):
+        @pl.when(i < groups)
+        def _():
+            def arrive(d, c):
+                @pl.when(d > 0)
+                def _():
+                    dispatch_copy(d).wait_recv()
+
+                return c
+
+            lax.fori_loop(i * sources, (i + 1) * sources, arrive, 0)
+
+            for way in range(2):
+                gather_copy(way, 1, i).start()
+
+        def gather_hop(hop, c):
+            d = i - hop + 1
+
+            @pl.when(jnp.logical_and(d >= 0, d < groups))
+            def _():
+                for way in range(2):
+                    gather_copy(way, hop - 1, d).wait_recv()
+                    gather_copy(way, hop, d).start()
+
+            return c
+
+        lax.fori_loop(2, shards, gather_hop, 0)
+
+        def sum_hop(hop, c):
+            d = i - last - hop + 1
+
+            @pl.when(jnp.logical_and(d >= 0, d < groups))
+            def _():
+                for way in range(2):
+                    sum_copy(way, hop - 1, d).wait_recv()
+                    sums[way, hop - 1, d] = (
+                        sums[way, hop - 1, d].astype(jnp.float32)
+                        + partial[sum_block(way, hop), d, way * half : (way + 1) * half].astype(
+                            jnp.float32
+                        )
+                    ).astype(jnp.bfloat16)
+                    sum_copy(way, hop, d).start()
+
+            return c
+
+        lax.fori_loop(2, shards, sum_hop, 0)
+        finished = i - 2 * last
+
+        @pl.when(finished >= 0)
+        def _():
+            for way in range(2):
+                sum_copy(way, last, finished).wait_recv()
+                done_out[finished, way * half : (way + 1) * half] = (
+                    sums[way, last, finished].astype(jnp.float32)
+                    + partial[me_t, finished, way * half : (way + 1) * half].astype(jnp.float32)
+                ).astype(jnp.bfloat16)
+
+            def leave(d, c):
+                @pl.when(d > 0)
+                def _():
+                    done_copy(d).start()
+
+                return c
+
+            lax.fori_loop(finished * sources, (finished + 1) * sources, leave, 0)
+
+        ready = i - last
+
+        @pl.when(jnp.logical_and(ready >= 0, ready < groups))
+        def _():
+            for way in range(2):
+                gather_copy(way, last, ready).wait_recv()
+
+            @pl.when(ready == 0)
+            def _():
+                for load in loads:
+                    load.wait()
+
+            expert(ready)
+            for way in range(2):
+                sums[way, 0, ready] = partial[
+                    sum_block(way, 1), ready, way * half : (way + 1) * half
+                ]
+                sum_copy(way, 1, ready).start()
+
+        return c
+
+    lax.fori_loop(0, groups + 2 * last, step, 0)
+
+    def combine(d, rows):
+        weights = jnp.where(slots == rank_ref[d], weight_ref[d], 0.0)
+        high = weights.astype(jnp.bfloat16)
+        low = (weights - high.astype(jnp.float32)).astype(jnp.bfloat16)
+        over_slots = (((0,), (0,)), ((), ()))
+        return lax.dot_general(
+            high, rows, over_slots, preferred_element_type=jnp.float32
+        ) + lax.dot_general(low, rows, over_slots, preferred_element_type=jnp.float32)
+
+    hidden[...] += combine(0, done_out[0, :capacity])
+
+    def take_done(d, c):
+        done_copy(d).wait_recv()
+        hidden[...] += combine(d, done_in[d])
+        return c
+
+    lax.fori_loop(1, experts, take_done, 0)
+    out_ref[...] = hidden[...].astype(jnp.bfloat16)
+
+    def finish_tp(d, c):
+        share_copy(d).wait_send()
+        square_copy(d).wait_send()
+        return c
+
+    lax.fori_loop(1, shards, finish_tp, 0)
+
+    def finish_sp(d, c):
+        dispatch_copy(d).wait_send()
+        done_copy(d).wait_send()
+        return c
+
+    lax.fori_loop(1, experts, finish_sp, 0)
+
+    def finish_chunk(d, c):
+        def finish_hop(hop, c):
+            for way in range(2):
+                gather_copy(way, hop, d).wait_send()
+                sum_copy(way, hop, d).wait_send()
+            return c
+
+        return lax.fori_loop(1, shards, finish_hop, c)
+
+    lax.fori_loop(0, groups, finish_chunk, 0)
+
+
+def tail_call(*operands):
+    *arrays, capacity = operands
+    shards, experts = lax.axis_size("tp"), lax.axis_size("sp")
+    length, width = arrays[4].shape
+    gate, up, down = arrays[8:]
+    sources = max(1, min(experts, 128 // capacity))
+    groups = experts // sources
+    rows = sources * capacity
+    bf16, f32 = jnp.bfloat16, jnp.float32
+    vmem = pl.BlockSpec(memory_space=pltpu.VMEM)
+    dma = pltpu.SemaphoreType.DMA
+    return pl.pallas_call(
+        functools.partial(tail_kernel, shards, experts),
+        out_shape=jax.ShapeDtypeStruct((length, width), bf16),
+        in_specs=[vmem] * 8 + [pl.BlockSpec(memory_space=pl.ANY)] * 3,
+        out_specs=vmem,
+        scratch_shapes=[
+            pltpu.VMEM(gate.shape, bf16),
+            pltpu.VMEM(up.shape, bf16),
+            pltpu.VMEM(down.shape, bf16),
+            pltpu.VMEM((shards, length, width), bf16),
+            pltpu.VMEM((shards, length, width), bf16),
+            pltpu.VMEM((8, length), f32),
+            pltpu.VMEM((shards, 8, length), f32),
+            pltpu.VMEM((length, width), f32),
+            pltpu.VMEM((length, width), bf16),
+            pltpu.VMEM((experts, capacity, width), bf16),
+            pltpu.VMEM((shards, groups, rows, width), bf16),
+            pltpu.VMEM((shards, groups, rows, width), bf16),
+            pltpu.VMEM((2, shards, groups, rows // 2, width), bf16),
+            pltpu.VMEM((groups, rows, width), bf16),
+            pltpu.VMEM((experts, capacity, width), bf16),
+            dma((3,)),
+            dma((shards,)),
+            dma((shards,)),
+            dma((shards,)),
+            dma((shards,)),
+            dma((experts,)),
+            dma((experts,)),
+            dma((2, shards, groups)),
+            dma((2, shards, groups)),
+            dma((2, shards, groups)),
+            dma((2, shards, groups)),
+            dma((experts,)),
+            dma((experts,)),
+        ],
+        compiler_params=pltpu.CompilerParams(
+            collective_id=0, has_side_effects=True, vmem_limit_bytes=56 * 1024 * 1024
+        ),
+    )(*arrays)
 
 
 def local(
@@ -241,72 +677,37 @@
         wide_output_gate,
         wide_norm_gain,
     )
-    partial_mix = jnp.dot(
-        narrow_head_output, narrow_output_rows, preferred_element_type=jnp.float32
-    )
-    partial_mix = partial_mix + jnp.dot(
-        wide_head_output, wide_output_rows, preferred_element_type=jnp.float32
-    )
-    mixed = lax.psum(partial_mix.astype(jnp.bfloat16), "tp").astype(jnp.float32)
-    hidden_state = resid.astype(jnp.float32) + mixed
-    normed = (
-        hidden_state
-        * lax.rsqrt(jnp.mean(hidden_state * hidden_state, axis=-1, keepdims=True) + NORM_EPS)
-        * feedforward_norm_gain
-    ).astype(jnp.bfloat16)
     experts = lax.axis_size("sp")
+    shards = lax.axis_size("tp")
     picks = routes.shape[1]
     capacity = 4 * length * picks // (3 * experts)
-    column_width = normed.shape[1] // lax.axis_size("tp")
+    width = resid.shape[1] // shards
     tp_index = lax.axis_index("tp")
-    flat_routes = routes.reshape(-1)
-    member_hits = (flat_routes[:, None] == jnp.arange(experts, dtype=jnp.int32)[None, :]).astype(
-        jnp.int32
-    )
-    ranks = jnp.sum((jnp.cumsum(member_hits, axis=0) - member_hits) * member_hits, axis=1)
-    slot_ids = flat_routes * capacity + ranks
-    source_rows = (
-        jnp.zeros((experts * capacity,), jnp.int32)
-        .at[slot_ids]
-        .set(jnp.arange(length * picks, dtype=jnp.int32) // picks)
-    )
-    occupied = jnp.zeros((experts * capacity,), jnp.int32).at[slot_ids].set(1)
-    gate_weight = expert_gate_matrix[0]
-    up_weight = expert_up_matrix[0]
-    down_weight = expert_down_matrix[0]
-    own_columns = lax.dynamic_slice_in_dim(normed, tp_index * column_width, column_width, 1)
-    outgoing = jnp.where(
-        occupied[:, None] > 0, own_columns[source_rows], jnp.zeros((), jnp.bfloat16)
-    )
-    arrived = lax.all_to_all(
-        outgoing.reshape(experts, capacity, column_width),
-        "sp",
-        split_axis=0,
-        concat_axis=0,
-        tiled=True,
-    )
-    slot_parts = arrived.reshape(experts * capacity, column_width)
-    piece = lax.all_gather(slot_parts, "tp", axis=1, tiled=True)
-    gate_pre = jnp.dot(piece, gate_weight, preferred_element_type=jnp.float32)
-    up_pre = jnp.dot(piece, up_weight, preferred_element_type=jnp.float32)
-    clamped = jnp.minimum(gate_pre, CLAMP_LIMIT)
-    act = (
-        (jnp.clip(up_pre, -CLAMP_LIMIT, CLAMP_LIMIT) + 1.0)
-        * clamped
-        * jax.nn.sigmoid(SIGMOID_SCALE * clamped)
-    ).astype(jnp.bfloat16)
-    partial_out = jnp.dot(act, down_weight, preferred_element_type=jnp.float32)
-    summed = lax.psum_scatter(
-        partial_out.reshape(experts, capacity, -1).astype(jnp.bfloat16),
-        "tp",
-        scatter_dimension=2,
-        tiled=True,
-    )
-    returned = lax.all_to_all(summed, "sp", split_axis=0, concat_axis=0, tiled=True)
-    token_rows = returned.reshape(experts * capacity, -1)[slot_ids].reshape(length, picks, -1)
-    combined = jnp.sum(token_rows.astype(jnp.float32) * routing_weight_values[..., None], axis=1)
-    own_state = lax.dynamic_slice_in_dim(hidden_state, tp_index * column_width, column_width, 1)
-    return (own_state + combined).astype(jnp.bfloat16)
+    expert_order = (lax.axis_index("sp") + jnp.arange(experts, dtype=jnp.int32)) % experts
+    hits = routes[None] == expert_order[:, None, None]
+    member = jnp.any(hits, axis=2)
+    weight_rows = jnp.sum(jnp.where(hits, routing_weight_values[None], 0.0), axis=2)
+    earlier = (jnp.arange(length)[:, None] < jnp.arange(length)[None, :]).astype(jnp.bfloat16)
+    ranks = jnp.dot(
+        member.astype(jnp.bfloat16), earlier, preferred_element_type=jnp.float32
+    ).astype(jnp.int32)
+    rank_rows = jnp.where(member, ranks, -1)
+    resid_own = lax.dynamic_slice_in_dim(resid, tp_index * width, width, 1)
+    gain_own = lax.dynamic_slice_in_dim(feedforward_norm_gain, tp_index * width, width, 0)
+    return tail_call(
+        narrow_head_output,
+        wide_head_output,
+        narrow_output_rows,
+        wide_output_rows,
+        resid_own,
+        gain_own[None, :],
+        rank_rows[:, None, :],
+        weight_rows[:, None, :],
+        expert_gate_matrix[0],
+        expert_up_matrix[0],
+        expert_down_matrix[0],
+        capacity,
+    )
 
 
 def solution(mesh):

time: 409 us -> 260 us (0.64)
  waiting for transfers between devices: 190 us -> 0.03 us
  Pallas kernels: 0 us -> 129 us
  blocking collectives: 62 us -> 31 us
  local copies, waits for them, and re-layouts: 56.8 us -> 31.5 us
  matrix products: 31.5 us -> 15.9 us
  other arithmetic: 33.6 us -> 23.6 us
  starting transfers between devices: 18 us -> 13.1 us
    pallas_call x0 -> x1, Pallas kernels: none -> 129 us  [tail_call(): pl.pallas_call(functools.partial(tail_kernel, shards, experts), out_shape...]
    psum x1 -> x0, waiting for transfers between devices: 60.3 us -> none  [local(): mixed = lax.psum(partial_mix.astype(jnp.bfloat16), 'tp').astype(jnp.float32)]
    reduce_scatter x1 -> x0, waiting for transfers between devices: 52.7 us -> none  [local(): lax.psum_scatter(partial_out.reshape(experts, capacity, -1).astype(jnp.bf...]
    all_gather x1 -> x0, waiting for transfers between devices: 50.3 us -> none  [local(): piece = lax.all_gather(slot_parts, 'tp', axis=1, tiled=True)]
    all_to_all x1 -> x0, blocking collectives: 31.1 us -> none  [local(): lax.all_to_all(outgoing.reshape(experts, capacity, column_width), 'sp', s...]
    all_to_all x1 -> x0, waiting for transfers between devices: 26.4 us -> none  [local(): lax.all_to_all(summed, 'sp', split_axis=0, concat_axis=0, tiled=True)]
    dot_general x5 -> x1, matrix products: 14.7 us -> 0.15 us  [local(): jnp.dot(member.astype(jnp.bfloat16), earlier, preferred_element_type=jnp....]
    gather x2 -> x0, local copies, waits for them, and re-layouts: 7.3 us -> none  [the longest x1 3.97 us: local(): own_columns[source_rows]]
  transfers between devices with their start and end apart: 9 -> 5, of which waited for: 4 -> 0; matrix products, arithmetic and copies ran while one was open for 18% -> 23% of each run, Pallas kernels for 0% -> 0%
where the time goes in v1:
time: 260 us; the launch traced here: 259 us
  Pallas kernels  129 us (50%)
  local copies, waits for them, and re-layouts  31.5 us (12%)
  blocking collectives  31 us (12%)
  other arithmetic  23.6 us (9%)
  matrix products  15.9 us (6%)
  between operations  14.8 us (6%)
  starting transfers between devices  13.1 us (5%)
    pallas_call x1, Pallas kernels, tail_call(): pl.pallas_call(functools.partial(tail_kernel, shards, experts), out_shape...  129 us
    all_gather x1, blocking collectives, entering_2(): lax.all_gather(a.astype(kind), axis)  17.4 us
    unnamed x1, blocking collectives  13.6 us
    ppermute x4, starting transfers between devices, passed_along(): return lax.ppermute(block, axis, route)  13.1 us
    dot_general x2, matrix products, pick_groups(): return jnp.einsum('sgn,hg->shn', grouped, chooser, precision=FULL_PRECISION)  5.77 us
    unnamed x88, local copies, waits for them, and re-layouts  5.47 us
  transfers between devices with their start and end apart: 5, of which 0 were waited for; matrix products, arithmetic and copies ran while one was open for 23% of the time, Pallas kernels for 0%

profile of v1, /device:TPU:0, one launch (start us, length us, event | category | flops | bytes accessed | tf_op | source)
XLA Modules:
  0.0 258.8 jit_solution(12994182193787594371)
XLA Ops:
  6.5 1.4 slice.150
  7.9 3.0 %collective-permute-start.1 = (bf16[3,512]{1,0:T(4,128)(2,1)}, bf16[3,512]{1,0:T(4,128)(2,1)}, u32[]{:S(2)}, u32[]{:S(2)}) collective-permute-start(bf16[3,512]{1,0:T(4,128)(2,1)} %slice.150), channel_id=1, source_target_pairs={{0,4},{4,8},{8,12},{12,16},{16,20},{20,24},{24,28},{1,5},{5,9},{9,... | collective-permute-start | bytes 9224 | tf_op jit(solution)/shard_map/ppermute | solution.py:26
  11.8 4.0 %collective-permute-start.2 = (bf16[3,256]{0,1:T(8,128)(2,1)S(1)}, bf16[3,256]{0,1:T(8,128)(2,1)S(1)}, u32[]{:S(2)}, u32[]{:S(2)}) collective-permute-start(bf16[3,256]{0,1:T(8,128)(2,1)S(1)} %copy.152), channel_id=1, source_target_pairs={{0,4},{4,8},{8,12},{12,16},{16,20},{20,24},{24,28},{1,5},{5,9},{9,... | collective-permute-start | bytes 4616 | tf_op jit(solution)/shard_map/ppermute | solution.py:26
  15.8 1.3 slice.176
  17.1 2.5 collective-permute-start.3
  19.5 1.3 slice.141
  20.8 3.6 %collective-permute-start = (bf16[3,512]{1,0:T(4,128)(2,1)}, bf16[3,512]{1,0:T(4,128)(2,1)}, u32[]{:S(2)}, u32[]{:S(2)}) collective-permute-start(bf16[3,512]{1,0:T(4,128)(2,1)} %slice.141), channel_id=1, source_target_pairs={{0,4},{4,8},{8,12},{12,16},{16,20},{20,24},{24,28},{1,5},{5,9},{9,... | collective-permute-start | bytes 9224 | tf_op jit(solution)/shard_map/ppermute | solution.py:26
  24.4 1.0 copy.153
  28.4 1.2 reduce_window_sum.34
  29.6 1.2 reduce_window_sum.36
  31.7 0.8 copy.165
  32.5 1.4 fusion.88
  34.5 0.8 fusion.92
  35.4 1.5 fusion.87
  37.0 1.5 fusion.86
  39.0 1.3 slice_bitcast_fusion.2
  40.4 1.1 convert_multiply_fusion
  42.1 0.8 compare_reduce_fusion
  43.0 0.8 fusion.67
  46.3 13.6 %all-reduce.2 = (bf16[32]{0:T(256)(128)(2,1)S(1)}, bf16[32]{0:T(256)(128)(2,1)S(1)}) all-reduce(bf16[32]{0:T(256)(128)(2,1)S(1)} %dynamic-update-slice, bf16[32]{0:T(256)(128)(2,1)S(1)} %dynamic-update-slice.1), channel_id=2, replica_groups=mesh['sp'=8,'tp'=4] {'sp'}, use_global_device_ids=true, to_apply=%add | all-reduce | flops 64 | bytes 256
  61.2 0.8 copy.155
  62.0 0.8 copy.177
  62.8 1.0 reshape.216
  63.8 0.8 copy.174
  64.5 1.3 dynamic_slice.45
  67.3 1.1 divide_multiply_fusion.3
  68.4 0.8 maximum_convert_fusion.1
  69.2 1.0 divide_multiply_fusion.1
  70.2 1.0 reshape.205
  72.0 1.0 divide_multiply_fusion
  73.6 2.9 %broadcast_multiply_fusion.3 = (f32[4,2,128,128]{3,0,2,1:T(4,128)S(1)}, f32[4,2,128,128]{3,0,2,1:T(4,128)}, f32[4,2,128,128]{3,0,2,1:T(4,128)}) fusion(f32[4,2,128]{0,2,1:T(8,128)S(1)} %copy-done.15, f32[4,2,128]{0,2,1:T(8,128)S(1)} %copy.158, f32[2,128,128,4]{2,3,1,0:T(4,128)} %bitcast.190, s32[4]{0:T(128)S(1)} %copy-done.38), kind=kOutput, calls=%fused_computation.114 | convolution fusion | flops 6553616 | bytes 2105360 | tf_op jit(solution)/shard_map/sgn,hg->shn/dot_general | solution.py:65
  76.4 1.0 convolution_bitcast_fusion
  77.4 3.1 %while.44 = (s32[]{:T(128)}, f32[4,128,128]{2,1,0:T(8,128)S(1)}, f32[2,4,128,128]{3,2,1,0:T(8,128)}, f32[2,4]{1,0:T(2,128)}, f32[2,4,128,128]{3,2,0,1:T(8,128)S(1)}, /*index=5*/s32[]{:T(128)}, s32[]{:T(128)}) while((s32[]{:T(128)}, f32[4,128,128]{2,1,0:T(8,128)S(1)}, f32[2,4,128,128]{3,2,1,0:T(8,128)}, f32[2,4]{1,0:T(2,128)}, ...), condition=%wide.region_8.9_spmd.clone, body=%wide.region_7.8_spmd.clone.sunk | while | flops 262147 | bytes 1311376 | solution.py:90
  81.2 1.7 convolution_bitcast_fusion.1
  83.0 3.4 %while.43 = (s32[]{:T(128)}, f32[4,128,64]{2,1,0:T(8,128)S(1)}, f32[2,4,128,64]{3,2,1,0:T(8,128)}, f32[2,4]{1,0:T(2,128)}, f32[2,4,128,64]{2,3,0,1:T(8,128)S(1)}, /*index=5*/s32[]{:T(128)}, s32[]{:T(128)}) while((s32[]{:T(128)}, f32[4,128,64]{2,1,0:T(8,128)S(1)}, f32[2,4,128,64]{3,2,1,0:T(8,128)}, f32[2,4]{1,0:T(2,128)}, ...), condition=%wide.region_2.3_spmd.clone, body=%wide.region_1.2_spmd.clone.sunk | while | flops 131075 | bytes 1311376 | solution.py:90
  86.4 1.0 maximum_convert_fusion
  87.5 1.1 divide_multiply_fusion.2
  88.6 1.0 reshape.204
  89.6 17.4 %all-gather.1 = bf16[32,128,64]{1,2,0:T(8,128)(2,1)} all-gather(bf16[4,128,64]{1,2,0:T(8,128)(2,1)S(1)} %copy.162), channel_id=3, replica_groups=mesh['sp'=8,'tp'=4] {'sp'}, dimensions={0}, use_global_device_ids=true | all-gather | bytes 589824 | tf_op jit(solution)/shard_map/all_gather | solution.py:32
  107.0 2.9 %broadcast_multiply_fusion.1 = (f32[4,2,128,128]{3,0,2,1:T(4,128)}, f32[4,2,128,128]{3,0,2,1:T(4,128)}, f32[4,2,128,128]{3,0,2,1:T(4,128)S(1)}) fusion(f32[4,2,128]{0,2,1:T(8,128)S(1)} %copy-done.14, f32[4,2,128]{0,2,1:T(8,128)S(1)} %copy-done.13, f32[2,128,128,4]{2,3,1,0:T(4,128)} %bitcast.191, s32[4]{0:T(128)S(1)} %copy-done.39), kind=kOutput, calls=%fused_computation.108 | convolution fusion | flops 6553616 | bytes 2105360 | tf_op jit(solution)/shard_map/sgn,hg->shn/dot_general | solution.py:65
  109.9 1.2 fusion.33
  111.2 1.6 fusion.36
  113.1 0.8 copy-done.5
  113.9 2.0 convolution_add_fusion
  116.7 1.1 fusion.26
  117.9 1.2 fusion.10
  121.6 128.6 %shard_map.235 = bf16[256,512]{1,0:T(8,128)(2,1)} custom-call(bf16[256,256]{1,0:T(8,128)(2,1)} %multiply_convert_fusion.narrow_ref, bf16[256,512]{1,0:T(8,128)(2,1)} %fusion.15.wide_ref, bf16[256,2048]{1,0:T(8,128)(2,1)} %narrow_rows_ref.1, bf16[512,2048]{1,0:T(8,128)(2,1)} %wide_rows_ref.1, bf16[256,512]{1,0:T(8,128)(2,1)} %constant_dynamic-slice_fusion.6.resid_ref, ...), custom_call_target="tpu_custom_call" | custom-call | tf_op jit(solution)/shard_map/pallas_call | solution.py:542
  250.3 1.7 copy.262
  (159 shorter events, 22.9 us)
Async XLA Ops:
  6.5 37.3 %copy-start = (bf16[256,2048]{1,0:T(8,128)(2,1)S(1)}, bf16[256,2048]{1,0:T(8,128)(2,1)}, u32[]{:S(2)}) copy-start(bf16[256,2048]{1,0:T(8,128)(2,1)} %param.31) | copy-start | bytes 3145732
  6.5 38.0 %copy-start.37 = (u32[32]{0:T(128)S(1)}, u32[32]{0:T(128)}, u32[]{:S(2)}) copy-start(u32[32]{0:T(128)} %constant.136) | copy-start | bytes 388
  6.5 57.2 %copy-start.12 = (bf16[256,256]{1,0:T(8,128)(2,1)S(1)}, bf16[256,256]{1,0:T(8,128)(2,1)}, u32[]{:S(2)}) copy-start(bf16[256,256]{1,0:T(8,128)(2,1)} %param.36) | copy-start | bytes 393220
  6.5 106.3 %all-gather.6.cloned.1.call-start = ((), (), s32[]{:S(2)}) async-start(), calls=%async_computation | async-start | bytes 1179648 | tf_op jit(solution)/shard_map/all_gather | solution.py:32
  7.9 60.5 %collective-permute-start.1 = (bf16[3,512]{1,0:T(4,128)(2,1)}, bf16[3,512]{1,0:T(4,128)(2,1)}, u32[]{:S(2)}, u32[]{:S(2)}) collective-permute-start(bf16[3,512]{1,0:T(4,128)(2,1)} %slice.150), channel_id=1, source_target_pairs={{0,4},{4,8},{8,12},{12,16},{16,20},{20,24},{24,28},{1,5},{5,9},{9,... | collective-permute-start | bytes 9224 | tf_op jit(solution)/shard_map/ppermute | solution.py:26
  11.8 55.3 %collective-permute-start.2 = (bf16[3,256]{0,1:T(8,128)(2,1)S(1)}, bf16[3,256]{0,1:T(8,128)(2,1)S(1)}, u32[]{:S(2)}, u32[]{:S(2)}) collective-permute-start(bf16[3,256]{0,1:T(8,128)(2,1)S(1)} %copy.152), channel_id=1, source_target_pairs={{0,4},{4,8},{8,12},{12,16},{16,20},{20,24},{24,28},{1,5},{5,9},{9,... | collective-permute-start | bytes 4616 | tf_op jit(solution)/shard_map/ppermute | solution.py:26
  17.1 54.1 %collective-permute-start.3 = (bf16[3,512]{1,0:T(4,128)(2,1)}, bf16[3,512]{1,0:T(4,128)(2,1)}, u32[]{:S(2)}, u32[]{:S(2)}) collective-permute-start(bf16[3,512]{1,0:T(4,128)(2,1)} %slice.176), channel_id=1, source_target_pairs={{0,4},{4,8},{8,12},{12,16},{16,20},{20,24},{24,28},{1,5},{5,9},{9,... | collective-permute-start | bytes 9224 | tf_op jit(solution)/shard_map/ppermute | solution.py:26
  20.8 65.6 %collective-permute-start = (bf16[3,512]{1,0:T(4,128)(2,1)}, bf16[3,512]{1,0:T(4,128)(2,1)}, u32[]{:S(2)}, u32[]{:S(2)}) collective-permute-start(bf16[3,512]{1,0:T(4,128)(2,1)} %slice.141), channel_id=1, source_target_pairs={{0,4},{4,8},{8,12},{12,16},{16,20},{20,24},{24,28},{1,5},{5,9},{9,... | collective-permute-start | bytes 9224 | tf_op jit(solution)/shard_map/ppermute | solution.py:26
  29.6 12.5 %copy-start.16 = (f32[4,2,128]{2,1,0:T(2,128)}, f32[4,2,128]{2,1,0:T(2,128)S(1)}, u32[]{:S(2)}) copy-start(f32[4,2,128]{2,1,0:T(2,128)S(1)} %reduce_window_sum.34) | copy-start | bytes 12292
  30.8 11.3 %copy-start.18 = (f32[4,2,128]{2,1,0:T(2,128)}, f32[4,2,128]{2,1,0:T(2,128)S(1)}, u32[]{:S(2)}) copy-start(f32[4,2,128]{2,1,0:T(2,128)S(1)} %reduce_window_sum.36) | copy-start | bytes 12292
  31.1 36.1 %copy-start.22 = (f32[4,2,1]{0,1,2:T(2,128)}, f32[4,2,1]{0,1,2:T(2,128)S(1)}, u32[]{:S(2)}) copy-start(f32[4,2,1]{0,1,2:T(2,128)S(1)} %copy.163) | copy-start | bytes 100
  31.3 11.6 %copy-start.21 = (f32[4,2,1]{0,1,2:T(2,128)}, f32[4,2,1]{0,1,2:T(2,128)S(1)}, u32[]{:S(2)}) copy-start(f32[4,2,1]{0,1,2:T(2,128)S(1)} %copy.156) | copy-start | bytes 100
  35.4 31.9 %copy-start.23 = (f32[1,256]{1,0:T(1,128)}, f32[1,256]{1,0:T(1,128)S(1)}, u32[]{:S(2)}) copy-start(f32[1,256]{1,0:T(1,128)S(1)} %get-tuple-element.341) | copy-start | bytes 3076
  35.4 31.9 %copy-start.25 = (f32[1,256]{1,0:T(1,128)}, f32[1,256]{1,0:T(1,128)S(1)}, u32[]{:S(2)}) copy-start(f32[1,256]{1,0:T(1,128)S(1)} %get-tuple-element.342) | copy-start | bytes 3076
  35.4 31.9 %copy-start.27 = (f32[1,256]{1,0:T(1,128)}, f32[1,256]{1,0:T(1,128)S(1)}, u32[]{:S(2)}) copy-start(f32[1,256]{1,0:T(1,128)S(1)} %get-tuple-element.343) | copy-start | bytes 3076
  35.4 31.9 %copy-start.29 = (f32[1,256]{1,0:T(1,128)}, f32[1,256]{1,0:T(1,128)S(1)}, u32[]{:S(2)}) copy-start(f32[1,256]{1,0:T(1,128)S(1)} %get-tuple-element.344) | copy-start | bytes 3076
  42.1 26.3 %copy-start.10 = (bf16[256,512]{1,0:T(8,128)(2,1)S(1)}, bf16[256,512]{1,0:T(8,128)(2,1)}, u32[]{:S(2)}) copy-start(bf16[256,512]{1,0:T(8,128)(2,1)} %param.34) | copy-start | bytes 786436
  68.4 2.8 %copy-start.11 = (bf16[256,512]{1,0:T(8,128)(2,1)S(1)}, bf16[256,512]{1,0:T(8,128)(2,1)}, u32[]{:S(2)}) copy-start(bf16[256,512]{1,0:T(8,128)(2,1)} %param.33) | copy-start | bytes 786436
  71.9 1.6 copy-start.15
  71.9 1.6 copy-start.38
  87.5 19.5 %copy-start.13 = (f32[4,2,128]{0,2,1:T(8,128)S(1)}, f32[4,2,128]{0,2,1:T(8,128)}, u32[]{:S(2)}) copy-start(f32[4,2,128]{0,2,1:T(8,128)} %copy.155) | copy-start | bytes 12292
  87.5 19.5 %copy-start.14 = (f32[4,2,128]{0,2,1:T(8,128)S(1)}, f32[4,2,128]{0,2,1:T(8,128)}, u32[]{:S(2)}) copy-start(f32[4,2,128]{0,2,1:T(8,128)} %copy.177) | copy-start | bytes 12292
  87.5 19.5 %copy-start.39 = (s32[4]{0:T(128)S(1)}, s32[4]{0:T(128)}, u32[]{:S(2)}) copy-start(s32[4]{0:T(128)} %and_select_fusion.1) | copy-start | bytes 52
  107.0 2.9 %copy-start.6 = (f32[4,2,128,128]{3,0,2,1:T(4,128)S(1)}, f32[4,2,128,128]{3,0,2,1:T(4,128)}, u32[]{:S(2)}) copy-start(f32[4,2,128,128]{3,0,2,1:T(4,128)} %get-tuple-element.349) | copy-start | bytes 1572868
  107.0 4.2 %copy-start.19 = (f32[4,2,128]{2,1,0:T(2,128)S(1)}, f32[4,2,128]{2,1,0:T(2,128)}, u32[]{:S(2)}) copy-start(f32[4,2,128]{2,1,0:T(2,128)} %copy-done.18) | copy-start | bytes 12292
  111.2 1.6 copy-start.1
  112.9 1.0 copy-start.5
  112.9 1.0 copy-start.31
  113.1 2.9 %copy-start.4 = (f32[256,4,128]{2,1,0:T(4,128)S(1)}, f32[256,4,128]{2,1,0:T(4,128)}, u32[]{:S(2)}) copy-start(f32[256,4,128]{2,1,0:T(4,128)} %reshape.216) | copy-start | bytes 1572868
  113.1 2.9 %copy-start.35 = (f32[4]{0:T(128)S(1)}, f32[4]{0:T(128)}, u32[]{:S(2)}) copy-start(f32[4]{0:T(128)} %get-tuple-element.345) | copy-start | bytes 52
  113.9 2.8 %copy-start.8 = (f32[2,4,128,64]{3,2,1,0:T(8,128)S(1)}, f32[2,4,128,64]{3,2,1,0:T(8,128)}, u32[]{:S(2)}) copy-start(f32[2,4,128,64]{3,2,1,0:T(8,128)} %get-tuple-element.153) | copy-start | bytes 786436
  113.9 2.8 %copy-start.9 = (f32[4,2,128,128]{3,0,2,1:T(4,128)S(1)}, f32[4,2,128,128]{3,0,2,1:T(4,128)}, u32[]{:S(2)}) copy-start(f32[4,2,128,128]{3,0,2,1:T(4,128)} %get-tuple-element.314) | copy-start | bytes 1572868
  113.9 2.8 %copy-start.32 = (f32[4,2]{0,1:T(2,128)S(1)}, f32[4,2]{0,1:T(2,128)}, u32[]{:S(2)}) copy-start(f32[4,2]{0,1:T(2,128)} %subtract_exponential_fusion.3) | copy-start | bytes 100
  115.9 2.0 copy-start.2
  115.9 2.0 copy-start.3
  115.9 2.0 copy-start.17
  115.9 2.0 copy-start.20
  116.6 2.6 copy-start.7
  116.6 2.6 copy-start.24
  116.6 2.6 copy-start.26
  116.6 2.6 copy-start.28
  116.6 2.6 copy-start.30
  116.6 2.6 copy-start.33
  119.1 1.1 copy-start.34
  119.2 1.7 copy-start.36
Sparse Core Ops, SparseCore 0:
  81.4 23.3 all-gather.5

commit v2 on v1

--- a/solution.py
+++ b/solution.py
@@ -26,26 +26,29 @@
     return lax.ppermute(block, axis, route)
 
 
-def entering_2(x, axis, join, neutral):
+def entering(narrow_parts, wide_parts, axis):
     place = lax.axis_index(axis)
-    gathered = jax.tree.map(
-        lambda a, kind: lax.all_gather(a.astype(kind), axis),
-        x,
-        jax.tree.map(lambda a: jnp.bfloat16 if a.dtype == jnp.float32 else a.dtype, x),
-    )
-    state = jax.tree.map(lambda a, e: jnp.zeros_like(a) + jnp.asarray(e, a.dtype), x, neutral)
-
-    def one(lap, state):
-        return join(
-            state,
-            jax.tree.map(
-                lambda a, own: lax.dynamic_index_in_dim(a, lap, 0, False).astype(own.dtype),
-                gathered,
-                x,
-            ),
-        )
-
-    return lax.fori_loop(0, place, one, state)
+    narrow_states, wide_states = narrow_parts[2], wide_parts[2]
+    heads, state_size, narrow_size = narrow_states.shape
+    totals = jnp.stack([narrow_parts[3], wide_parts[3]], axis=1)
+    total_rows = jnp.broadcast_to(
+        jnp.repeat(totals, 4, axis=1)[:, :, None], (heads, 8, narrow_size)
+    )
+    narrow_packed = jnp.concatenate([narrow_states, total_rows], axis=1).astype(jnp.bfloat16)
+    narrow_all, wide_all = lax.all_gather((narrow_packed, wide_states.astype(jnp.bfloat16)), axis)
+    count = narrow_all.shape[0]
+    earlier = jnp.arange(count) < place
+    between = jnp.logical_and(
+        jnp.arange(count)[:, None] < jnp.arange(count)[None, :], earlier[None, :]
+    )
+
+    def carry(states, row):
+        decay = narrow_all[:, :, state_size + row, 0].astype(jnp.float32)
+        gap = jnp.sum(jnp.where(between[:, :, None], decay[None], 0.0), axis=1)
+        factor = jnp.where(earlier[:, None], jnp.exp(gap), 0.0)
+        return jnp.sum(factor[:, :, None, None] * states.astype(jnp.float32), axis=0)
+
+    return carry(narrow_all[:, :, :state_size], 0), carry(wide_all, 4)
 
 
 def conv_with_rim(values, rim_rows, weight):
@@ -55,14 +58,6 @@
     for tap_index in range(weight.shape[0]):
         accumulated = accumulated + weight[tap_index] * padded[tap_index : tap_index + length]
     return jax.nn.silu(accumulated)
-
-
-def pick_groups(channel_table, first_head, head_count):
-    length = channel_table.shape[0]
-    grouped = channel_table.reshape(length, GROUPS, -1)
-    owners = (first_head + jnp.arange(head_count, dtype=jnp.int32)) // (HEADS // GROUPS)
-    chooser = (owners[:, None] == jnp.arange(GROUPS, dtype=jnp.int32)[None, :]).astype(jnp.float32)
-    return jnp.einsum("sgn,hg->shn", grouped, chooser, precision=FULL_PRECISION)
 
 
 def local_head(values, step_logarithm, key_head_rows, query_head_rows, block_len):
@@ -126,7 +121,7 @@
     step_logarithm = -jnp.exp(decay_vector)[None, :] * step_length_values + position_decay_rows
     values = mixed_input_rows * step_length_values[..., None]
     walker = functools.partial(local_head, block_len=BLOCK)
-    return jax.vmap(walker, in_axes=(1, 1, 1, 1))(
+    return jax.vmap(walker, in_axes=(1, 1, None, None))(
         values, step_logarithm, key_head_rows, query_head_rows
     )
 
@@ -134,15 +129,6 @@
 def finish_group(parts, carried_states):
     return jax.vmap(finish_head, in_axes=(0, 0, 0, 0, 0, 0), out_axes=1)(
         parts[0], parts[1], parts[4], parts[5], parts[6], carried_states
-    )
-
-
-def chain_combine(earlier, later):
-    return (
-        earlier[0] + later[0],
-        earlier[1] + later[1],
-        jnp.exp(later[0])[:, None, None] * earlier[2] + later[2],
-        jnp.exp(later[1])[:, None, None] * earlier[3] + later[3],
     )
 
 
@@ -610,29 +596,34 @@
     length = resid.shape[0]
     head_count = narrow_head_input.shape[1] // NARROW_HEAD_DIM
     rim_len = narrow_conv_taps.shape[0] - 1
-    rim_rows = passed_along(
-        (
-            narrow_head_input[length - rim_len :],
-            wide_head_input[length - rim_len :],
-            key_group_input[length - rim_len :],
-            query_group_input[length - rim_len :],
-        ),
-        "sp",
-        1,
-    )
+    first_head = lax.axis_index("tp") * head_count
+    state_size = key_group_input.shape[1] // GROUPS
+    group_column = first_head // (HEADS // GROUPS) * state_size
+
+    def own_group(table):
+        return lax.dynamic_slice_in_dim(table, group_column, state_size, 1)
+
+    streams = (
+        narrow_head_input,
+        wide_head_input,
+        own_group(key_group_input),
+        own_group(query_group_input),
+    )
+    rims = passed_along(
+        jnp.concatenate([stream[length - rim_len :] for stream in streams], axis=1), "sp", 1
+    )
+    edges = [0]
+    for stream in streams:
+        edges.append(edges[-1] + stream.shape[1])
+    rim_rows = [rims[:, low:high] for low, high in zip(edges[:-1], edges[1:])]
     narrow_head_mix = conv_with_rim(narrow_head_input, rim_rows[0], narrow_conv_taps).reshape(
         length, head_count, NARROW_HEAD_DIM
     )
     wide_head_mix = conv_with_rim(wide_head_input, rim_rows[1], wide_conv_taps).reshape(
         length, head_count, WIDE_HEAD_DIM
     )
-    first_head = lax.axis_index("tp") * head_count
-    key_head_rows = pick_groups(
-        conv_with_rim(key_group_input, rim_rows[2], key_conv_taps), first_head, head_count
-    )
-    query_head_rows = pick_groups(
-        conv_with_rim(query_group_input, rim_rows[3], query_conv_taps), first_head, head_count
-    )
+    key_head_rows = conv_with_rim(streams[2], rim_rows[2], own_group(key_conv_taps))
+    query_head_rows = conv_with_rim(streams[3], rim_rows[3], own_group(query_conv_taps))
     step_length_values = jax.nn.softplus(step_input_rows.astype(jnp.float32))
     narrow_parts = head_pieces_list(
         narrow_head_mix,
@@ -650,19 +641,7 @@
         key_head_rows,
         query_head_rows,
     )
-    summary = (narrow_parts[3], wide_parts[3], narrow_parts[2], wide_parts[2])
-    carried = entering_2(
-        summary,
-        "sp",
-        chain_combine,
-        (
-            jnp.zeros_like(summary[0]),
-            jnp.zeros_like(summary[1]),
-            jnp.zeros_like(summary[2]),
-            jnp.zeros_like(summary[3]),
-        ),
-    )
-    narrow_carry, wide_carry = (carried[2], carried[3])
+    narrow_carry, wide_carry = entering(narrow_parts, wide_parts, "sp")
     narrow_head_output = group_out(
         finish_group(narrow_parts, narrow_carry),
         narrow_head_mix,

time: 260 us -> 215 us (0.83)
  Pallas kernels: 129 us -> 111 us
  waiting for transfers between devices: 0.03 us -> 13.5 us
  blocking collectives: 31 us -> 18.4 us
  starting transfers between devices: 13.1 us -> 2.41 us
  local copies, waits for them, and re-layouts: 31.5 us -> 21.9 us
  matrix products: 15.9 us -> 9.09 us
    pallas_call x1, Pallas kernels: 129 us -> 111 us  [tail_call(): pl.pallas_call(functools.partial(tail_kernel, shards, experts), out_shape...]
    unnamed x1 -> x0, blocking collectives: 13.6 us -> none
    all_gather x1, waiting for transfers between devices: 0.01 us -> 13.5 us  [entering(): lax.all_gather((narrow_packed, wide_states.astype(jnp.bfloat16)), axis)]
    ppermute x4 -> x1, starting transfers between devices: 13.1 us -> 2.41 us  [passed_along(): return lax.ppermute(block, axis, route)]
    dot_general x2 -> x0, matrix products: 5.77 us -> none  [pick_groups(): return jnp.einsum('sgn,hg->shn', grouped, chooser, precision=FULL_PRECISION)]
    slice x4 -> x2, local copies, waits for them, and re-layouts: 5.19 us -> 1.7 us  [conv_with_rim(): weight[tap_index] * padded[tap_index:tap_index + length]]
    mul x4, other arithmetic: 4.24 us -> 1.62 us  [conv_with_rim(): return jax.nn.silu(accumulated)]
    unnamed x88 -> x63, local copies, waits for them, and re-layouts: 5.47 us -> 3.57 us
  transfers between devices with their start and end apart: 5 -> 2, of which waited for: 0 -> 1; matrix products, arithmetic and copies ran while one was open for 23% -> 14% of each run, Pallas kernels for 0% -> 0%
where the time goes in v2:
time: 215 us; the launch traced here: 214 us
  Pallas kernels  111 us (52%)
  other arithmetic  23.1 us (11%)
  local copies, waits for them, and re-layouts  21.9 us (10%)
  blocking collectives  18.4 us (9%)
  between operations  14.1 us (7%)
  waiting for transfers between devices  13.5 us (6%)
  matrix products  9.09 us (4%)
  starting transfers between devices  2.41 us (1%)
    pallas_call x1, Pallas kernels, tail_call(): pl.pallas_call(functools.partial(tail_kernel, shards, experts), out_shape...  111 us
    all_gather x1, blocking collectives, entering(): lax.all_gather((narrow_packed, wide_states.astype(jnp.bfloat16)), axis)  18.4 us
    all_gather x1, waiting for transfers between devices, entering(): lax.all_gather((narrow_packed, wide_states.astype(jnp.bfloat16)), axis)  13.5 us
  transfers between devices with their start and end apart: 2, of which 1 were waited for; matrix products, arithmetic and copies ran while one was open for 14% of the time, Pallas kernels for 0%

profile of v2, /device:TPU:0, one launch (start us, length us, event | category | flops | bytes accessed | tf_op | source)
XLA Modules:
  0.0 214.1 jit_solution(10420105761537303697)
XLA Ops:
  6.6 0.9 dynamic-slice.1
  7.4 0.8 dynamic-slice
  8.2 0.7 slice.163
  8.9 0.7 slice.162
  9.8 2.4 %collective-permute-start = (bf16[3,1024]{0,1:T(8,128)(2,1)S(1)}, bf16[3,1024]{0,1:T(8,128)(2,1)S(1)}, u32[]{:S(2)}, u32[]{:S(2)}) collective-permute-start(bf16[3,1024]{0,1:T(8,128)(2,1)S(1)} %copy.183), channel_id=1, source_target_pairs={{0,4},{4,8},{8,12},{12,16},{16,20},{20,24},{24,28},{1,5},{5,9},{9,... | collective-permute-start | bytes 18440 | tf_op jit(solution)/shard_map/ppermute | solution.py:26
  12.2 1.5 constant_dynamic-slice_fusion.5
  13.7 0.8 negate_bitcast_fusion
  14.5 0.7 compare_select_fusion.1
  15.2 0.8 fusion.74
  16.0 1.2 reduce_window_sum.34
  17.3 1.2 reduce_window_sum.36
  19.7 1.3 slice_bitcast_fusion.2
  21.7 0.7 constant_dynamic-slice_fusion.4
  23.0 0.8 fusion.88
  24.4 1.1 convert_multiply_fusion.1
  25.5 0.9 fusion.84
  27.1 0.8 compare_reduce_fusion
  28.0 0.8 fusion.69
  28.8 0.7 constant_dynamic-slice_fusion.3.resid_ref
  30.0 0.8 copy.201
  30.7 1.0 reshape.267
  31.9 1.4 dynamic_slice.38
  36.0 0.7 copy-done.2
  36.7 1.1 convolution_bitcast_fusion.1
  37.8 2.0 while.26
  37.8 0.7 bitcast_dynamic-update-slice_fusion.4
  38.8 0.7 bitcast_dynamic-update-slice_fusion.4
  39.9 18.4 %all_gather.10 = bf16[8,4,136,64]{2,3,1,0:T(8,128)(2,1)S(1)} all-gather(bf16[1,4,136,64]{2,3,1,0:T(8,128)(2,1)S(1)} %pad_maximum_fusion), channel_id=1, replica_groups=mesh['sp'=8,'tp'=4] {'sp'}, dimensions={0}, use_global_device_ids=true | all-gather | bytes 626688 | tf_op jit(solution)/shard_map/all_gather | solution.py:38
  59.4 0.8 multiply_reduce_fusion
  60.3 0.9 slice.235
  62.2 0.7 convolution_bitcast_fusion
  62.9 3.0 %while.27 = (s32[]{:T(128)}, f32[4,128,128]{2,1,0:T(8,128)S(1)}, f32[2,4,128,128]{3,2,1,0:T(8,128)}, f32[2,4]{1,0:T(2,128)}, f32[2,4,128,128]{3,2,0,1:T(8,128)S(1)}, /*index=5*/s32[]{:T(128)}, s32[]{:T(128)}) while((s32[]{:T(128)}, f32[4,128,128]{2,1,0:T(8,128)S(1)}, f32[2,4,128,128]{3,2,1,0:T(8,128)}, f32[2,4]{1,0:T(2,128)}, ...), condition=%wide.region_11.12_spmd.clone, body=%wide.region_10.11_spmd.clone.sunk | while | flops 262147 | bytes 1310876 | solution.py:85
  63.0 0.7 bitcast_dynamic-update-slice_fusion.5
  63.7 0.6 fusion.96
  64.5 0.8 bitcast_dynamic-update-slice_fusion.5
  66.0 0.7 convert_element_type.81
  66.7 0.9 maximum_convert_fusion.2
  67.8 0.8 divide_multiply_fusion.3
  68.9 2.3 %fusion.15 = f32[4,2,128,64]{2,3,1,0:T(8,128)S(1)} fusion(f32[4,2,128]{2,1,0:T(2,128)} %get-tuple-element.203, f32[2,128,128]{2,1,0:T(8,128)S(1)} %bitcast.172, f32[2,4,128,64]{3,2,1,0:T(8,128)} %get-tuple-element.61, f32[4,128,64]{2,1,0:T(8,128)S(1)} %copy.198, f32[4,2]{0,1:T(2,128)} %subtract_exponential_fusion.3), kind=kOutput, calls=%fused_computation.38 | convolution fusion | flops 100925440 | bytes 790560 | tf_op jit(solution)/shard_map/vmap(bln,bnp->blp)/dot_general | solution.py:92
  71.3 1.2 fusion.5
  73.3 0.7 multiply_convert_fusion.narrow_ref
  74.0 1.5 fusion.20
  75.5 13.5 %all-gather.3.cloned.1.call-done = bf16[32,128,128]{2,1,0:T(8,128)(2,1)} async-done(((bf16[4,128,128]{2,1,0:T(8,128)(2,1)}), bf16[32,128,128]{2,1,0:T(8,128)(2,1)}) %all-gather.3.cloned.1.call-update) | async-done | bytes 1048592 | tf_op jit(solution)/shard_map/all_gather | solution.py:38
  89.0 1.6 fusion.4
  90.6 1.8 convolution_add_fusion
  93.4 0.7 fusion.10.wide_ref
  94.1 111.4 %shard_map.235 = bf16[256,512]{1,0:T(8,128)(2,1)} custom-call(bf16[256,256]{1,0:T(8,128)(2,1)} %multiply_convert_fusion.narrow_ref, bf16[256,512]{1,0:T(8,128)(2,1)} %fusion.10.wide_ref, bf16[256,2048]{1,0:T(8,128)(2,1)} %narrow_rows_ref.1, bf16[512,2048]{1,0:T(8,128)(2,1)} %wide_rows_ref.1, bf16[256,512]{1,0:T(8,128)(2,1)} %constant_dynamic-slice_fusion.3.resid_ref, ...), custom_call_target="tpu_custom_call" | custom-call | tf_op jit(solution)/shard_map/pallas_call | solution.py:528
  205.5 1.7 copy.271
  (141 shorter events, 13.3 us)
Async XLA Ops:
  6.5 22.2 %copy-start = (bf16[256,2048]{1,0:T(8,128)(2,1)S(1)}, bf16[256,2048]{1,0:T(8,128)(2,1)}, u32[]{:S(2)}) copy-start(bf16[256,2048]{1,0:T(8,128)(2,1)} %param.29) | copy-start | bytes 3145732
  6.5 23.0 %copy-start.10 = (bf16[256,256]{1,0:T(8,128)(2,1)S(1)}, bf16[256,256]{1,0:T(8,128)(2,1)}, u32[]{:S(2)}) copy-start(bf16[256,256]{1,0:T(8,128)(2,1)} %param.30) | copy-start | bytes 393220
  6.5 23.4 %copy-start.11 = (bf16[256,256]{1,0:T(8,128)(2,1)S(1)}, bf16[256,256]{1,0:T(8,128)(2,1)}, u32[]{:S(2)}) copy-start(bf16[256,256]{1,0:T(8,128)(2,1)} %param.34) | copy-start | bytes 393220
  6.5 82.5 %all-gather.3.cloned.1.call-start = ((), (), s32[]{:S(2)}) async-start(), calls=%async_computation | async-start | bytes 1179648 | tf_op jit(solution)/shard_map/all_gather | solution.py:38
  9.8 24.6 %collective-permute-start = (bf16[3,1024]{0,1:T(8,128)(2,1)S(1)}, bf16[3,1024]{0,1:T(8,128)(2,1)S(1)}, u32[]{:S(2)}, u32[]{:S(2)}) collective-permute-start(bf16[3,1024]{0,1:T(8,128)(2,1)S(1)} %copy.183), channel_id=1, source_target_pairs={{0,4},{4,8},{8,12},{12,16},{16,20},{20,24},{24,28},{1,5},{5,9},{9,... | collective-permute-start | bytes 18440 | tf_op jit(solution)/shard_map/ppermute | solution.py:26
  15.2 20.8 %copy-start.14 = (f32[256,4]{0,1:T(4,128)}, f32[256,4]{0,1:T(4,128)S(1)}, u32[]{:S(2)}) copy-start(f32[256,4]{0,1:T(4,128)S(1)} %get-tuple-element.194) | copy-start | bytes 12292
  19.6 10.1 %copy-start.13 = (f32[4,2,1]{0,1,2:T(2,128)}, f32[4,2,1]{0,1,2:T(2,128)S(1)}, u32[]{:S(2)}) copy-start(f32[4,2,1]{0,1,2:T(2,128)S(1)} %copy.206) | copy-start | bytes 100
  23.8 11.7 %copy-start.16 = (f32[1,256]{1,0:T(1,128)}, f32[1,256]{1,0:T(1,128)S(1)}, u32[]{:S(2)}) copy-start(f32[1,256]{1,0:T(1,128)S(1)} %get-tuple-element.207) | copy-start | bytes 3076
  23.8 11.7 %copy-start.18 = (f32[1,256]{1,0:T(1,128)}, f32[1,256]{1,0:T(1,128)S(1)}, u32[]{:S(2)}) copy-start(f32[1,256]{1,0:T(1,128)S(1)} %get-tuple-element.208) | copy-start | bytes 3076
  23.8 11.7 %copy-start.20 = (f32[1,256]{1,0:T(1,128)}, f32[1,256]{1,0:T(1,128)S(1)}, u32[]{:S(2)}) copy-start(f32[1,256]{1,0:T(1,128)S(1)} %get-tuple-element.209) | copy-start | bytes 3076
  23.8 11.7 %copy-start.22 = (f32[1,256]{1,0:T(1,128)}, f32[1,256]{1,0:T(1,128)S(1)}, u32[]{:S(2)}) copy-start(f32[1,256]{1,0:T(1,128)S(1)} %get-tuple-element.210) | copy-start | bytes 3076
  34.4 1.6 copy-start.9
  36.0 0.7 copy-start.2
  39.8 21.5 %copy-start.8 = (bf16[256,512]{1,0:T(8,128)(2,1)S(1)}, bf16[256,512]{1,0:T(8,128)(2,1)}, u32[]{:S(2)}) copy-start(bf16[256,512]{1,0:T(8,128)(2,1)} %param.31) | copy-start | bytes 786436
  62.9 4.6 %copy-start.4 = (f32[4,128,64]{1,2,0:T(8,128)S(1)}, f32[4,128,64]{1,2,0:T(8,128)}, u32[]{:S(2)}) copy-start(f32[4,128,64]{1,2,0:T(8,128)} %multiply_reduce_fusion) | copy-start | bytes 393220
  66.0 5.2 %copy-start.3 = (f32[256,256]{0,1:T(8,128)S(1)}, f32[256,256]{0,1:T(8,128)}, u32[]{:S(2)}) copy-start(f32[256,256]{0,1:T(8,128)} %copy-done.2) | copy-start | bytes 786436
  66.0 6.5 %copy-start.7 = (bf16[256,256]{0,1:T(8,128)(2,1)S(1)}, bf16[256,256]{0,1:T(8,128)(2,1)}, u32[]{:S(2)}) copy-start(bf16[256,256]{0,1:T(8,128)(2,1)} %copy.201) | copy-start | bytes 393220
  67.7 3.5 %copy-start.12 = (pred[128,128]{1,0:T(8,128)(4,1)S(1)}, pred[128,128]{1,0:T(8,128)(4,1)}, u32[]{:S(2)}) copy-start(pred[128,128]{1,0:T(8,128)(4,1)} %iota_compare_fusion.2) | copy-start | bytes 49156
  67.7 3.5 %copy-start.15 = (f32[256,4]{0,1:T(4,128)S(1)}, f32[256,4]{0,1:T(4,128)}, u32[]{:S(2)}) copy-start(f32[256,4]{0,1:T(4,128)} %copy-done.14) | copy-start | bytes 12292
  67.7 4.8 %copy-start.17 = (f32[1,256]{1,0:T(1,128)S(1)}, f32[1,256]{1,0:T(1,128)}, u32[]{:S(2)}) copy-start(f32[1,256]{1,0:T(1,128)} %copy-done.16) | copy-start | bytes 3076
  67.7 4.8 %copy-start.19 = (f32[1,256]{1,0:T(1,128)S(1)}, f32[1,256]{1,0:T(1,128)}, u32[]{:S(2)}) copy-start(f32[1,256]{1,0:T(1,128)} %copy-done.18) | copy-start | bytes 3076
  67.7 4.8 %copy-start.21 = (f32[1,256]{1,0:T(1,128)S(1)}, f32[1,256]{1,0:T(1,128)}, u32[]{:S(2)}) copy-start(f32[1,256]{1,0:T(1,128)} %copy-done.20) | copy-start | bytes 3076
  67.7 4.8 %copy-start.23 = (f32[1,256]{1,0:T(1,128)S(1)}, f32[1,256]{1,0:T(1,128)}, u32[]{:S(2)}) copy-start(f32[1,256]{1,0:T(1,128)} %copy-done.22) | copy-start | bytes 3076
  67.7 4.8 %copy-start.25 = (f32[4]{0:T(128)S(1)}, f32[4]{0:T(128)}, u32[]{:S(2)}) copy-start(f32[4]{0:T(128)} %get-tuple-element.220) | copy-start | bytes 52
  68.9 3.6 %copy-start.5 = (f32[2,128,128]{2,1,0:T(8,128)}, f32[2,128,128]{2,1,0:T(8,128)S(1)}, u32[]{:S(2)}) copy-start(f32[2,128,128]{2,1,0:T(8,128)S(1)} %fusion.89) | copy-start | bytes 393220
  71.2 2.0 copy-start.24
  71.2 2.1 copy-start.28
  72.6 1.4 copy-start.6
  74.0 18.4 %copy-start.27 = (f32[4]{0:T(128)S(1)}, f32[4]{0:T(128)}, u32[]{:S(2)}) copy-start(f32[4]{0:T(128)} %get-tuple-element.219) | copy-start | bytes 52
  75.5 16.9 %copy-start.1 = (f32[256,4,128]{2,1,0:T(4,128)S(1)}, f32[256,4,128]{2,1,0:T(4,128)}, u32[]{:S(2)}) copy-start(f32[256,4,128]{2,1,0:T(4,128)} %reshape.267) | copy-start | bytes 1572868
  92.4 1.0 copy-start.26
Sparse Core Ops, SparseCore 0:
  66.8 22.1 all-gather.2
